TPU v7x, 128 devices: a whole 4x4x4 slice. The times are simulated.
128 devices in a mesh: sp: 32 (over z, y, core), tp: 4 (over x).
Axes of the slice: x: 4, y: 4, z: 4, core: 2. Of those that a mesh axis runs over, the one named last changes fastest.
Arguments:
- tokens: bfloat16 [8192, 4096], P(('sp', 'tp')), may hold values from -700 to 700
- down_query: bfloat16 [4096, 1024], replicated, may hold values from -0.09375 to 0.09375
- down_latent: bfloat16 [4096, 512], replicated, may hold values from -0.09375 to 0.09375
- down_rotary: bfloat16 [4096, 64], replicated, may hold values from -0.09375 to 0.09375
- query_gain: float32 [1024], replicated, may hold values from 0.1 to 1.9
- latent_gain: float32 [512], replicated, may hold values from 0.1 to 1.9
- up_query: bfloat16 [1024, 2048], P(None, 'tp'), may hold values from -0.1875 to 0.1875
- up_query_rotary: bfloat16 [1024, 1024], P(None, 'tp'), may hold values from -0.1875 to 0.1875
- up_key: bfloat16 [512, 2048], P(None, 'tp'), may hold values from -0.25 to 0.25
- up_value: bfloat16 [512, 2048], P(None, 'tp'), may hold values from -0.25 to 0.25
- out_weight: bfloat16 [2048, 4096], P('tp'), may hold values from -0.39648438 to 0.39648438
Outputs:
- mixed: bfloat16 [8192, 4096], P(('sp', 'tp'))
All inputs are finite; a program needn't handle non-finite values.
Results may differ from a plain program's by a relative error of at most 0.03.
Values may be sent and summed in bfloat16 or wider, within the bound.
A program may use at most 192 MiB of HBM per device.

v0:
```python
import jax
import jax.numpy as jnp
from jax import lax
from jax.sharding import PartitionSpec as P

NOPE = 128
ROPE = 64
VDIM = 128


rope_base = 500000.0
norm_eps = 1e-06
masked_score = -1e30


def sent_together(arrays, axis, dim, along):
    both = jnp.concatenate(arrays, axis=along)
    filled, at, outs = (lax.all_gather(both, axis, axis=dim, tiled=True), 0, [])
    for a in arrays:
        outs.append(lax.slice_in_dim(filled, at, at + a.shape[along], axis=along))
        at += a.shape[along]
    return tuple(outs)


def rotate_half(values, positions):
    half = values.shape[-1] // 2
    inverse = rope_base ** (-jnp.arange(0, 2 * half, 2, dtype=jnp.float32) / (2 * half))
    angles = positions.astype(jnp.float32)[:, None] * inverse
    if values.ndim == 3:
        angles = angles[:, None, :]
    cosine = jnp.cos(angles)
    sine = jnp.sin(angles)
    first = values[..., :half]
    second = values[..., half:]
    return jnp.concatenate(
        [first * cosine - second * sine, second * cosine + first * sine], axis=-1
    )


def norm_rows(values, gain):
    return values * lax.rsqrt(jnp.mean(values * values, axis=-1, keepdims=True) + norm_eps) * gain


def local(
    tokens,
    down_query,
    down_latent,
    down_rotary,
    query_gain,
    latent_gain,
    up_query,
    up_query_rotary,
    up_key,
    up_value,
    out_weight,
):
    own_count = tokens.shape[0]
    seq_index = lax.axis_index("sp")
    own_start = (seq_index * lax.axis_size("tp") + lax.axis_index("tp")) * own_count
    own_positions = own_start + jnp.arange(own_count, dtype=jnp.int32)
    query_latent = norm_rows(
        jnp.dot(tokens, down_query, preferred_element_type=jnp.float32), query_gain
    ).astype(jnp.bfloat16)
    kv_latent = norm_rows(
        jnp.dot(tokens, down_latent, preferred_element_type=jnp.float32), latent_gain
    ).astype(jnp.bfloat16)
    key_rotary = rotate_half(
        jnp.dot(tokens, down_rotary, preferred_element_type=jnp.float32), own_positions
    ).astype(jnp.bfloat16)
    query_rows, latent_rows, rotary_rows = sent_together(
        (query_latent, kv_latent, key_rotary), "tp", 0, 1
    )
    span = query_rows.shape[0]
    heads = up_key.shape[1] // NOPE
    query_positions = seq_index * span + jnp.arange(span, dtype=jnp.int32)
    last_position = seq_index * span + span - 1
    query_plain = (
        jnp.dot(query_rows, up_query, preferred_element_type=jnp.float32)
        .astype(jnp.bfloat16)
        .reshape(span, heads, NOPE)
    )
    query_turned = rotate_half(
        jnp.dot(query_rows, up_query_rotary, preferred_element_type=jnp.float32).reshape(
            span, heads, ROPE
        ),
        query_positions,
    ).astype(jnp.bfloat16)
    factor = (NOPE + ROPE) ** (-0.5)
    start_state = (
        jnp.full((heads, span), masked_score, jnp.float32),
        jnp.zeros((heads, span), jnp.float32),
        jnp.zeros((span, heads, VDIM), jnp.float32),
    )
    pieces = sent_together((latent_rows, rotary_rows), "sp", 0, 1)

    def make_keys():
        latent_piece, turned_piece = pieces
        key_count = latent_piece.shape[0]
        key_plain = (
            jnp.dot(latent_piece, up_key, preferred_element_type=jnp.float32)
            .astype(jnp.bfloat16)
            .reshape(key_count, heads, NOPE)
        )
        key_values = (
            jnp.dot(latent_piece, up_value, preferred_element_type=jnp.float32)
            .astype(jnp.bfloat16)
            .reshape(key_count, heads, VDIM)
        )
        return (key_plain, key_values, turned_piece)

    def update(state):
        best, total, summed = state
        key_plain, key_values, key_turned = make_keys()
        key_count = key_plain.shape[0]
        key_positions = jnp.arange(key_count, dtype=jnp.int32)
        scores = jnp.einsum(
            "qhd,khd->hqk", query_plain, key_plain, preferred_element_type=jnp.float32
        )
        scores = scores + jnp.einsum(
            "qhr,kr->hqk", query_turned, key_turned, preferred_element_type=jnp.float32
        )
        scores = scores * factor
        allowed = (key_positions[None, :] <= query_positions[:, None])[None]
        scores = jnp.where(allowed, scores, masked_score)
        new_best = jnp.maximum(best, jnp.max(scores, axis=-1))
        weights = jnp.where(allowed, jnp.exp(scores - new_best[..., None]), 0.0)
        total = jnp.sum(weights, axis=-1)
        added = jnp.einsum(
            "hqk,khd->qhd",
            weights.astype(jnp.bfloat16),
            key_values,
            preferred_element_type=jnp.float32,
        )
        summed = added
        return (new_best, total, summed)

    def keep(state):
        return state

    best, total, summed = lax.cond(jnp.int32(0) <= last_position, update, keep, start_state)
    attended = (
        (summed / jnp.transpose(total)[:, :, None]).astype(jnp.bfloat16).reshape(span, heads * VDIM)
    )
    return lax.psum_scatter(
        jnp.dot(attended, out_weight, preferred_element_type=jnp.float32).astype(jnp.bfloat16),
        "tp",
        scatter_dimension=0,
        tiled=True,
    )


def solution(mesh):
    return jax.shard_map(
        local,
        mesh=mesh,
        in_specs=(
            P(("sp", "tp"), None),
            P(),
            P(),
            P(),
            P(),
            P(),
            P(None, "tp"),
            P(None, "tp"),
            P(None, "tp"),
            P(None, "tp"),
            P("tp", None),
        ),
        out_specs=P(("sp", "tp"), None),
        check_vma=False,
    )
```

profile of v0, /device:TPU:96, one launch (start us, length us, event | category | flops | bytes accessed | tf_op | source)
XLA Modules:
  0.0 236.0 jit_solution(14751858438894699339)
XLA Ops:
  6.6 1.6 fusion.30
  8.1 0.1 fusion.28
  8.3 0.1 copy.23
  8.6 5.4 %multiply_reduce_fusion = (f32[64]{0:T(128)S(1)}, f32[64,1024]{1,0:T(8,128)S(1)}) fusion(bf16[64,4096]{1,0:T(8,128)(2,1)} %param.13, bf16[4096,1024]{1,0:T(8,128)(2,1)} %param.14), kind=kOutput, calls=%fused_computation.30 | convolution fusion | flops 537001920 | bytes 9175296 | tf_op jit(solution)/shard_map/dot_general | solution.py:62
  14.0 0.9 multiply_reduce_fusion.1
  15.2 13.8 %all_gather.6 = bf16[256,1600]{1,0:T(8,128)(2,1)S(1)} all-gather(bf16[64,1600]{1,0:T(8,128)(2,1)S(1)} %concatenate.13), channel_id=1, replica_groups=mesh['sp'=32,'tp'=4] {'tp'}, dimensions={0}, use_global_device_ids=true | all-gather | bytes 1024000 | tf_op jit(solution)/shard_map/all_gather | solution.py:18
  29.0 0.8 concatenate.16
  29.8 0.2 reduce-scatter.2.cloned.1.call-start
  30.0 0.2 multiply_cosine_fusion
  30.2 0.3 fusion.18
  30.7 0.4 convolution_convert_fusion.3
  31.1 57.7 %all-gather.2.cloned.1.call-done = bf16[8192,576]{1,0:T(8,128)(2,1)} async-done(((bf16[256,576]{1,0:T(8,128)(2,1)}), bf16[8192,576]{1,0:T(8,128)(2,1)}) %all-gather.2.cloned.1.call-update) | async-done | bytes 9437200 | tf_op jit(solution)/shard_map/all_gather | solution.py:18
  88.8 104.7 %conditional.1 = (f32[4,256]{1,0:T(4,128)S(1)}, f32[256,4,128]{0,2,1:T(8,128)}) conditional(s32[]{:T(128)} %convert_element_type.43, () %tuple.13, (s32[]{:T(128)}, s32[256]{0:T(256)S(1)}, bf16[8192,576]{1,0:T(8,128)(2,1)}, bf16[512,512]{1,0:T(8,128)(2,1)}, bf16[256,512]{1,0:T(8,128)(2,1)S(1)}, /*index=5*/bf16[256,4,64]{0,2,1:T(8,128)(2,1)S(1)}, ...), branch_computations={%region_2.0_spmd, %region_3.6_spmd} | conditional | flops 14053014528 | bytes 252603472 | solution.py:140
  88.8 13.3 %copy.25 = bf16[8192,576]{0,1:T(8,128)(2,1)} copy(bf16[8192,576]{1,0:T(8,128)(2,1)} %get-tuple-element.49) | data formatting | bytes 18874368 | tf_op jit(solution)/shard_map
  102.1 10.2 %convolution_convert_fusion.1 = bf16[8192,512]{0,1:T(8,128)(2,1)} fusion(bf16[512,512]{1,0:T(8,128)(2,1)S(1)} %copy-done.7, bf16[8192,576]{0,1:T(8,128)(2,1)} %copy.25), kind=kOutput, calls=%fused_computation.11 | convolution fusion | flops 4299161600 | bytes 17301504 | tf_op jit(solution)/shard_map/cond/branch_1_fun/dot_general | solution.py:100
  112.3 15.3 %fusion.14 = f32[4,8192,256]{2,1,0:T(8,128)} fusion(bf16[8192,4,128]{0,2,1:T(8,128)(2,1)} %bitcast.42, bf16[256,512]{1,0:T(8,128)(2,1)S(1)} %get-tuple-element.29), kind=kOutput, calls=%fused_computation.17 | convolution fusion | flops 2147483648 | bytes 42205184 | tf_op jit(solution)/shard_map/cond/branch_1_fun/qhd,khd->hqk/dot_general | solution.py:116
  127.6 1.4 iota_compare_fusion
  129.0 22.8 %fusion.29 = (f32[4,256]{1,0:T(4,128)S(1)}, f32[4,256,8192]{1,2,0:T(8,128)}) fusion(bf16[256,4,64]{0,2,1:T(8,128)(2,1)S(1)} %get-tuple-element.30, bf16[8192,576]{0,1:T(8,128)(2,1)} %copy.25, f32[4,8192,256]{2,1,0:T(8,128)} %fusion.14, pred[256,8192]{0,1:T(8,128)(4,1)S(1)} %iota_compare_fusion), kind=kOutput, calls=%fused_computation.53 | convolution fusion | flops 1107295232 | bytes 70389760 | tf_op jit(solution)/shard_map/cond/branch_1_fun/qhr,kr->hqk/dot_general | solution.py:119
  151.9 10.2 %convolution_convert_fusion = bf16[8192,512]{0,1:T(8,128)(2,1)} fusion(bf16[512,512]{1,0:T(8,128)(2,1)S(1)} %copy-done.8, bf16[8192,576]{0,1:T(8,128)(2,1)} %copy.25), kind=kOutput, calls=%fused_computation.10 | convolution fusion | flops 4299161600 | bytes 17301504 | tf_op jit(solution)/shard_map/cond/branch_1_fun/dot_general | solution.py:105
  162.1 17.4 %fusion.11 = f32[256,4,128]{0,2,1:T(8,128)} fusion(bf16[8192,4,128]{0,2,1:T(8,128)(2,1)} %bitcast.46, f32[4,256,8192]{1,2,0:T(8,128)} %get-tuple-element.55, f32[4,256]{1,0:T(4,128)S(1)} %broadcast_maximum_fusion, pred[256,8192]{0,1:T(8,128)(4,1)S(1)} %iota_compare_fusion), kind=kOutput, calls=%fused_computation.15 | convolution fusion | flops 2172649472 | bytes 44568576 | tf_op jit(solution)/shard_map/cond/branch_1_fun/hqk,khd->qhd/dot_general | solution.py:128
  179.5 14.0 %fusion.3 = f32[4,256]{1,0:T(4,128)S(1)} fusion(f32[4,256,8192]{1,2,0:T(8,128)} %get-tuple-element.55, f32[4,256]{1,0:T(4,128)S(1)} %broadcast_maximum_fusion, pred[256,8192]{0,1:T(8,128)(4,1)S(1)} %iota_compare_fusion), kind=kLoop, calls=%fused_computation.5 | loop fusion | flops 25164800 | bytes 35659776 | tf_op jit(solution)/shard_map/cond/branch_1_fun/reduce_sum | solution.py:127
  193.5 1.2 divide_convert_fusion
  194.6 4.8 %convolution_convert_fusion.2 = bf16[256,4096]{1,0:T(8,128)(2,1)} fusion(bf16[256,512]{0,1:T(8,128)(2,1)S(1)} %bitcast.43, bf16[512,4096]{1,0:T(8,128)(2,1)} %param.23), kind=kOutput, calls=%fused_computation.23 | convolution fusion | flops 1074790400 | bytes 6553600 | tf_op jit(solution)/shard_map/dot_general | solution.py:145
  199.5 29.7 %reduce-scatter.2.cloned.1.call-done = bf16[64,4096]{1,0:T(8,128)(2,1)} async-done(((bf16[256,4096]{1,0:T(8,128)(2,1)}), bf16[64,4096]{1,0:T(8,128)(2,1)}) %reduce-scatter.2.cloned.1.call-update) | async-done | bytes 524304 | tf_op jit(solution)/shard_map/reduce_scatter | solution.py:144
  (35 shorter events, 0.5 us)
Async XLA Ops:
  6.5 24.1 %copy-start = (bf16[1024,512]{1,0:T(8,128)(2,1)S(1)}, bf16[1024,512]{1,0:T(8,128)(2,1)}, u32[]{:S(2)}) copy-start(bf16[1024,512]{1,0:T(8,128)(2,1)} %param.19) | copy-start | bytes 3145732
  6.5 82.2 %all-gather.2.cloned.1.call-start = ((), (), s32[]{:S(2)}) async-start(), calls=%async_computation.1 | async-start | bytes 10813440 | tf_op jit(solution)/shard_map/all_gather | solution.py:18
  8.5 5.4 %copy-start.2 = (bf16[64,4096]{1,0:T(8,128)(2,1)S(1)}, bf16[64,4096]{1,0:T(8,128)(2,1)}, u32[]{:S(2)}) copy-start(bf16[64,4096]{1,0:T(8,128)(2,1)} %param.13) | copy-start | bytes 1572868
  8.5 5.4 %copy-start.3 = (bf16[4096,512]{1,0:T(8,128)(2,1)S(1)}, bf16[4096,512]{1,0:T(8,128)(2,1)}, u32[]{:S(2)}) copy-start(bf16[4096,512]{1,0:T(8,128)(2,1)} %param.15) | copy-start | bytes 12582916
  8.5 6.4 %copy-start.5 = (f32[1024]{0:T(1024)S(1)}, f32[1024]{0:T(1024)}, u32[]{:S(2)}) copy-start(f32[1024]{0:T(1024)} %param.17) | copy-start | bytes 12292
  8.5 6.5 %copy-start.6 = (f32[512]{0:T(512)S(1)}, f32[512]{0:T(512)}, u32[]{:S(2)}) copy-start(f32[512]{0:T(512)} %param.18) | copy-start | bytes 6148
  8.5 21.7 %copy-start.4 = (bf16[1024,256]{1,0:T(8,128)(2,1)S(1)}, bf16[1024,256]{1,0:T(8,128)(2,1)}, u32[]{:S(2)}) copy-start(bf16[1024,256]{1,0:T(8,128)(2,1)} %param.20) | copy-start | bytes 1572868
  29.8 199.4 %reduce-scatter.2.cloned.1.call-start = ((), (), s32[]{:S(2)}) async-start(), calls=%async_computation.2 | async-start | bytes 2621440 | tf_op jit(solution)/shard_map/reduce_scatter | solution.py:144
  88.8 13.3 %copy-start.7 = (bf16[512,512]{1,0:T(8,128)(2,1)S(1)}, bf16[512,512]{1,0:T(8,128)(2,1)}, u32[]{:S(2)}) copy-start(bf16[512,512]{1,0:T(8,128)(2,1)} %get-tuple-element.38) | copy-start | bytes 1572868 | tf_op jit(solution)/shard_map/cond
  129.0 22.9 %copy-start.8 = (bf16[512,512]{1,0:T(8,128)(2,1)S(1)}, bf16[512,512]{1,0:T(8,128)(2,1)}, u32[]{:S(2)}) copy-start(bf16[512,512]{1,0:T(8,128)(2,1)} %get-tuple-element.39) | copy-start | bytes 1572868 | tf_op jit(solution)/shard_map/cond
  193.5 35.7 %copy-start.1 = (bf16[1024,512]{1,0:T(8,128)(2,1)S(1)}, bf16[1024,512]{1,0:T(8,128)(2,1)}, u32[]{:S(2)}) copy-start(bf16[1024,512]{1,0:T(8,128)(2,1)} %param.19) | copy-start | bytes 3145732
Sparse Core Ops, SparseCore 0:
  29.9 58.8 all-gather.1
  199.6 29.5 reduce-scatter.1
where the time goes:
time: 239 us; the launch traced here: 236 us
  matrix products  89.4 us (37%)
  waiting for transfers between devices  87.4 us (37%)
  other arithmetic  17.1 us (7%)
  local copies, waits for them, and re-layouts  14.4 us (6%)
  blocking collectives  13.8 us (6%)
  between operations  13.6 us (6%)
    all_gather x1, waiting for transfers between devices, sent_together(): filled, at, outs = (lax.all_gather(both, axis, axis=dim, tiled=True), 0, [])  57.7 us
    reduce_scatter x1, waiting for transfers between devices, local(): lax.psum_scatter(jnp.dot(attended, out_weight, preferred_element_type=jnp...  29.7 us
    dot_general x1, matrix products, update(): jnp.einsum('qhr,kr->hqk', query_turned, key_turned, preferred_element_typ...  22.8 us
    dot_general x1, matrix products, update(): jnp.einsum('hqk,khd->qhd', weights.astype(jnp.bfloat16), key_values, pref...  17.4 us
    dot_general x1, matrix products, update(): jnp.einsum('qhd,khd->hqk', query_plain, key_plain, preferred_element_type...  15.3 us
    reduce_sum x1, other arithmetic, update(): total = jnp.sum(weights, axis=-1)  14 us
    all_gather x1, blocking collectives, sent_together(): filled, at, outs = (lax.all_gather(both, axis, axis=dim, tiled=True), 0, [])  13.8 us
    another operation x3, local copies, waits for them, and re-layouts  13.5 us
  transfers between devices with their start and end apart: 2, of which 2 were waited for; matrix products, arithmetic and copies ran while one was open for 0% of the time, Pallas kernels for 0%

commit v1 on v0

v1 whole, which is shorter than its diff:
```python
import functools

import jax
import jax.numpy as jnp
from jax import lax
from jax.experimental import pallas as pl
from jax.experimental.pallas import tpu as pltpu
from jax.sharding import PartitionSpec as P

NOPE = 128
ROPE = 64
VDIM = 128
HEADS = 4
OWN = 64
GROUP = 256
BLOCK = 288
VROWS = 144
RING = 4

rope_base = 500000.0
norm_eps = 1e-06
masked_score = -1e30

f32 = jnp.float32
bf16 = jnp.bfloat16
MESH = pl.DeviceIdType.MESH

X_MSG, A_MSG, B_MSG, Q_MSG, QX_MSG, OX_MSG, R_MSG = 0, 4, 8, 24, 28, 29, 30
COLS = 4
N_MSG = R_MSG + 6 * COLS

UNIT_OA = ((0, 0, -1, 1, -1, 2, 0, -1), (1, 0, 2, 1, -1, 2, 1, 2))
UNIT_OB = ((0, 1, 0, 1, 1, 1, 2, 2), (0, -1, 0, -1, -1, -1, 2, 2))


def pick(index, values):
    out = jnp.int32(values[0])
    for i, v in enumerate(values[1:], 1):
        out = jnp.where(index == i, jnp.int32(v), out)
    return out


def mod4(v):
    return lax.rem(v + 8, 4)


def kernel(
    tokens,
    down_query,
    down_latent,
    down_rotary,
    query_gain,
    latent_gain,
    up_query,
    up_query_rotary,
    up_key,
    up_value,
    out_weight,
    key_cos,
    key_sin,
    query_cos,
    query_sin,
    out,
    wdl,
    wdr,
    wdq,
    wuq,
    wur,
    wuk,
    wuv,
    wout,
    lat,
    ql,
    qt,
    uvt,
    kbuf,
    vbuf,
    acc,
    best,
    xsend,
    xrecv,
    pbuf,
    r1buf,
    dbuf,
    cbuf,
    crecv,
    local_sem,
    ssem,
    rsem,
):
    sp = lax.axis_index("sp")
    x = lax.axis_index("tp")
    c = lax.rem(sp, 2)
    m = sp // 2
    y = lax.rem(m, 4)
    z = m // 4
    first = c == 0
    a = jnp.where(first, y, z)
    b = jnp.where(first, z, y)
    stride_a = jnp.where(first, 2, 8)
    stride_b = jnp.where(first, 8, 2)

    def at(aa, bb):
        return {"sp": aa * stride_a + bb * stride_b + c, "tp": x}

    xp, xm, x2 = mod4(x + 1), mod4(x - 1), mod4(x + 2)
    dev_xp = {"sp": sp, "tp": xp}
    dev_xm = {"sp": sp, "tp": xm}
    dev_ap, dev_am = at(mod4(a + 1), b), at(mod4(a - 1), b)
    dev_bp, dev_bm = at(a, mod4(b + 1)), at(a, mod4(b - 1))
    dev_core = {"sp": sp + 1 - 2 * c, "tp": x}

    def copy_in(i, src, dst):
        return pltpu.make_async_copy(src, dst, local_sem.at[i])

    K4 = 1024
    loads = []
    for k in range(4):
        rows = pl.ds(k * K4, K4)
        loads.append(copy_in(k, down_latent.at[rows], wdl.at[rows]))
    loads.append(copy_in(4, down_rotary, wdr))
    for k in range(4):
        rows = pl.ds(k * K4, K4)
        loads.append(copy_in(5 + k, down_query.at[rows], wdq.at[rows]))
    loads.append(copy_in(9, up_query, wuq))
    loads.append(copy_in(10, up_query_rotary, wur))
    loads.append(copy_in(11, up_key, wuk))
    loads.append(copy_in(12, up_value, wuv))
    loads.append(copy_in(13, out_weight, wout))
    for load in loads:
        load.start()

    barrier = pltpu.get_barrier_semaphore()
    for dev in (dev_xp, dev_xm, dev_ap, dev_am, dev_bp, dev_bm, dev_core):
        pl.semaphore_signal(barrier, inc=1, device_id=dev, device_id_type=MESH)

    def rcopy(i, src, dst, dev):
        return pltpu.make_async_remote_copy(
            src_ref=src,
            dst_ref=dst,
            send_sem=ssem.at[i],
            recv_sem=rsem.at[i],
            device_id=dev,
            device_id_type=MESH,
        )

    def same(i, ref, dev):
        return rcopy(i, ref, ref, dev)

    def group(aa, bb):
        return mod4(bb) * 4 + mod4(aa)

    s0 = group(a, b)
    lo, hi = pl.ds(0, BLOCK // 2), pl.ds(BLOCK // 2, BLOCK // 2)
    xs_lo, xs_hi = pl.ds(0, 2), pl.ds(2, 2)

    send = {}
    recv = {}

    def both(i, sent, received, dev):
        send[i] = same(i, sent, dev)
        recv[i] = same(i, received, dev)

    both(X_MSG, lat.at[s0, x], lat.at[s0, xm], dev_xp)
    both(X_MSG + 1, lat.at[s0, x], lat.at[s0, xp], dev_xm)
    both(X_MSG + 2, lat.at[s0, xm, lo], lat.at[s0, x2, lo], dev_xp)
    both(X_MSG + 3, lat.at[s0, xp, hi], lat.at[s0, x2, hi], dev_xm)
    both(A_MSG, lat.at[s0], lat.at[group(a - 1, b)], dev_ap)
    both(A_MSG + 1, lat.at[s0], lat.at[group(a + 1, b)], dev_am)
    both(A_MSG + 2, lat.at[group(a - 1, b), xs_lo], lat.at[group(a + 2, b), xs_lo], dev_ap)
    both(A_MSG + 3, lat.at[group(a + 1, b), xs_hi], lat.at[group(a + 2, b), xs_hi], dev_am)
    for k, o in enumerate((0, 1, -1, 2)):
        i = B_MSG + 4 * k
        own, lower, upper, far = (group(a + o, b + d) for d in (0, -1, 1, 2))
        both(i, lat.at[own], lat.at[lower], dev_bp)
        both(i + 1, lat.at[own], lat.at[upper], dev_bm)
        both(i + 2, lat.at[lower, xs_lo], lat.at[far, xs_lo], dev_bp)
        both(i + 3, lat.at[upper, xs_hi], lat.at[far, xs_hi], dev_bm)
    q_lo, q_hi = pl.ds(0, OWN // 2), pl.ds(OWN // 2, OWN // 2)
    both(Q_MSG, ql.at[x], ql.at[xm], dev_xp)
    both(Q_MSG + 1, ql.at[x], ql.at[xp], dev_xm)
    both(Q_MSG + 2, ql.at[xm, q_lo], ql.at[x2, q_lo], dev_xp)
    both(Q_MSG + 3, ql.at[xp, q_hi], ql.at[x2, q_hi], dev_xm)
    send[QX_MSG] = same(QX_MSG, qt.at[c], dev_core)
    recv[QX_MSG] = same(QX_MSG, qt.at[1 - c], dev_core)
    send[OX_MSG] = rcopy(OX_MSG, xsend, xrecv, dev_core)
    recv[OX_MSG] = send[OX_MSG]

    def start(*ids):
        for i in ids:
            send[i].start()

    def arrived(*ids):
        for i in ids:
            recv[i].wait_recv()

    def norm_rows(values, gain):
        return values * lax.rsqrt(jnp.mean(values * values, axis=-1, keepdims=True) + norm_eps) * gain

    latent = jnp.zeros((OWN, 512), f32)
    for k in range(4):
        loads[k].wait()
        cols = slice(k * K4, (k + 1) * K4)
        latent = latent + jnp.dot(tokens[:, cols], wdl[cols, :], preferred_element_type=f32)
    latent = norm_rows(latent, latent_gain[...]).astype(bf16)
    for t in range(4):
        lat[s0, x, t * OWN : (t + 1) * OWN, :] = latent[:, t * 128 : (t + 1) * 128]
    loads[4].wait()
    turned = jnp.dot(tokens[...], wdr[...], preferred_element_type=f32)
    turned = jnp.concatenate([turned, turned], axis=-1)
    turned = turned * key_cos[...] + pltpu.roll(turned, 32, 1) * key_sin[...]
    lane = lax.broadcasted_iota(jnp.int32, (32, 128), 1)
    lat[s0, x, 256:288, :] = jnp.where(lane < 64, turned[:32], turned[32:]).astype(bf16)

    pl.semaphore_wait(barrier, 7)
    start(X_MSG, X_MSG + 1)

    query = jnp.zeros((OWN, 1024), f32)
    for k in range(4):
        loads[5 + k].wait()
        cols = slice(k * K4, (k + 1) * K4)
        query = query + jnp.dot(tokens[:, cols], wdq[cols, :], preferred_element_type=f32)
    ql[x] = norm_rows(query, query_gain[...]).astype(bf16)

    arrived(X_MSG, X_MSG + 1)
    start(X_MSG + 2, X_MSG + 3, Q_MSG, Q_MSG + 1)
    for i in range(9, 14):
        loads[i].wait()
    uvt[...] = jnp.transpose(wuv[...].astype(f32)).astype(bf16)
    for h in range(HEADS):
        vbuf[h, VDIM:VROWS, :] = jnp.ones((VROWS - VDIM, 2 * GROUP), bf16)
    acc[...] = jnp.zeros_like(acc)
    best[...] = jnp.full(best.shape, masked_score, f32)
    arrived(X_MSG + 2, X_MSG + 3)
    start(A_MSG, A_MSG + 1, B_MSG, B_MSG + 1)
    arrived(Q_MSG, Q_MSG + 1)
    start(Q_MSG + 2, Q_MSG + 3)
    arrived(Q_MSG + 2, Q_MSG + 3)

    factor = (NOPE + ROPE) ** (-0.5) * 1.4426950408889634
    rows = ql[...].reshape(GROUP, 1024)
    plain = jnp.dot(rows, wuq[...], preferred_element_type=f32) * factor
    qt[c, 0 : HEADS * NOPE, :] = jnp.transpose(plain).astype(bf16)
    turned = jnp.transpose(jnp.dot(rows, wur[...], preferred_element_type=f32) * factor)
    cosine, sine = query_cos[...], query_sin[...]
    for h in range(HEADS):
        one = turned[h * ROPE : h * ROPE + 32]
        two = turned[h * ROPE + 32 : (h + 1) * ROPE]
        at_row = HEADS * NOPE + h * ROPE
        qt[c, at_row : at_row + 32, :] = (one * cosine - two * sine).astype(bf16)
        qt[c, at_row + 32 : at_row + 64, :] = (two * cosine + one * sine).astype(bf16)
    start(QX_MSG)
    arrived(QX_MSG)

    UNIT = 2 * GROUP

    def attend(set_one, set_two, m_one, m_two, masked):
        parts, rots = [], []
        for s in (set_one, set_two):
            tiles = [
                lat[s, :, t * OWN : (t + 1) * OWN, :].reshape(GROUP, 128) for t in range(4)
            ]
            parts.append(jnp.concatenate(tiles, axis=1))
            packed = lat[s, :, 256:288, :]
            swapped = pltpu.roll(packed.reshape(128, 128).astype(f32), 64, 1).astype(bf16)
            rots.append(
                jnp.concatenate([packed, swapped.reshape(4, 32, 128)], axis=1).reshape(GROUP, 128)
            )
        latents = jnp.concatenate(parts, axis=0)
        keys = jnp.dot(latents, wuk[...], preferred_element_type=f32).astype(bf16)
        for h in range(HEADS):
            kbuf[h, :, 0:NOPE] = keys[:, h * NOPE : (h + 1) * NOPE]
            kbuf[h, :, NOPE:256] = jnp.concatenate(rots, axis=0)
        values = lax.dot_general(
            uvt[...], latents, (((1,), (1,)), ((), ())), preferred_element_type=f32
        ).astype(bf16)
        for h in range(HEADS):
            vbuf[h, 0:VDIM, :] = values[h * VDIM : (h + 1) * VDIM]

        def head(h, carry):
            key = kbuf[h]
            value = vbuf[h]
            for j in range(2):
                at_plain = pl.multiple_of(h * NOPE, NOPE)
                at_turned = pl.multiple_of(HEADS * NOPE + h * ROPE, ROPE)
                queries = jnp.concatenate(
                    [
                        qt[j, pl.ds(at_plain, NOPE), :],
                        qt[j, pl.ds(at_turned, ROPE), :],
                        jnp.zeros((ROPE, GROUP), bf16),
                    ],
                    axis=0,
                )
                scores = jnp.dot(key, queries, preferred_element_type=f32)
                if masked:
                    row = lax.broadcasted_iota(jnp.int32, (UNIT, GROUP), 0)
                    col = lax.broadcasted_iota(jnp.int32, (UNIT, GROUP), 1)
                    base_one = (2 * m_one + c) * GROUP
                    base_two = (2 * m_two + c) * GROUP - GROUP
                    place = row + jnp.where(row < GROUP, base_one, base_two)
                    scores = jnp.where(
                        place <= col + (2 * m + j) * GROUP, scores, masked_score
                    )
                old = best[j, h]
                new = jnp.maximum(old, jnp.max(scores, axis=0, keepdims=True))
                weights = jnp.exp2(scores - new).astype(bf16)
                best[j, h] = new
                acc[j, h] = acc[j, h] * jnp.exp2(old - new) + jnp.dot(
                    value, weights, preferred_element_type=f32
                )
            return carry

        lax.fori_loop(0, HEADS, head, 0)

    def unit(u, carry):
        @pl.when(u == 0)
        def _():
            arrived(A_MSG, A_MSG + 1)
            start(A_MSG + 2, A_MSG + 3)
            start(B_MSG + 4, B_MSG + 5, B_MSG + 8, B_MSG + 9)

        @pl.when(u == 1)
        def _():
            arrived(B_MSG, B_MSG + 1)
            start(B_MSG + 2, B_MSG + 3)

        @pl.when(u == 2)
        def _():
            arrived(A_MSG + 2, A_MSG + 3)
            start(B_MSG + 12, B_MSG + 13)

        for k in (1, 2, 3):

            @pl.when(u == 2 + k)
            def _(k=k):
                arrived(B_MSG + 4 * k, B_MSG + 4 * k + 1)
                start(B_MSG + 4 * k + 2, B_MSG + 4 * k + 3)

        @pl.when(u == 6)
        def _():
            arrived(B_MSG + 2, B_MSG + 3, B_MSG + 6, B_MSG + 7)

        @pl.when(u == 7)
        def _():
            arrived(B_MSG + 10, B_MSG + 11, B_MSG + 14, B_MSG + 15)

        sets, spots = [], []
        for n in range(2):
            aa = mod4(a + pick(u, UNIT_OA[n]))
            bb = mod4(b + pick(u, UNIT_OB[n]))
            sets.append(bb * 4 + aa)
            spots.append(jnp.where(first, bb * 4 + aa, aa * 4 + bb))
        plain_unit = jnp.logical_and(spots[0] < m, spots[1] < m)
        some = jnp.logical_or(spots[0] <= m, spots[1] <= m)

        @pl.when(plain_unit)
        def _():
            attend(*sets, *spots, False)

        @pl.when(jnp.logical_and(some, jnp.logical_not(plain_unit)))
        def _():
            attend(*sets, *spots, True)

        return carry

    lax.fori_loop(0, 8, unit, 0)

    other = 1 - c
    for h in range(HEADS):
        xsend[h, 0:136, :] = acc[other, h, 0:136, :]
        xsend[h, 136:144, :] = jnp.broadcast_to(best[other, h], (8, GROUP))
    start(OX_MSG)
    arrived(OX_MSG)
    heads = []
    for h in range(HEADS):
        mine, theirs = best[c, h], xrecv[h, 136:137, :]
        top = jnp.maximum(mine, theirs)
        w_mine, w_theirs = jnp.exp2(mine - top), jnp.exp2(theirs - top)
        total = acc[c, h, 128:129, :] * w_mine + xrecv[h, 128:129, :] * w_theirs
        summed = acc[c, h, 0:128, :] * w_mine + xrecv[h, 0:128, :] * w_theirs
        heads.append(jnp.transpose(summed / total).astype(bf16))
    attended = jnp.concatenate(heads, axis=1)

    WIDE = 4096 // COLS
    top, low = pl.ds(0, 32), pl.ds(32, 32)
    for k in range(COLS):
        cols = pl.ds(k * WIDE, WIDE)
        i = R_MSG + 6 * k
        send[i] = rcopy(i, pbuf.at[x2, top, cols], r1buf.at[0, :, cols], dev_xp)
        send[i + 1] = rcopy(i + 1, pbuf.at[x2, low, cols], r1buf.at[1, :, cols], dev_xm)
        send[i + 2] = rcopy(i + 2, pbuf.at[xp, low, cols], dbuf.at[0, :, cols], dev_xp)
        send[i + 3] = rcopy(i + 3, pbuf.at[xm, top, cols], dbuf.at[1, :, cols], dev_xm)
        send[i + 4] = rcopy(i + 4, cbuf.at[0, :, cols], crecv.at[0, :, cols], dev_xp)
        send[i + 5] = rcopy(i + 5, cbuf.at[1, :, cols], crecv.at[1, :, cols], dev_xm)
        for n in range(6):
            recv[i + n] = send[i + n]
    for k in range(COLS):
        cols = slice(k * WIDE, (k + 1) * WIDE)
        part = jnp.dot(attended, wout[:, cols], preferred_element_type=f32).astype(bf16)
        pbuf[:, :, cols] = part.reshape(4, OWN, WIDE)
        start(R_MSG + 6 * k, R_MSG + 6 * k + 1)
    for k in range(COLS):
        start(R_MSG + 6 * k + 2, R_MSG + 6 * k + 3)
    for k in range(COLS):
        cols = slice(k * WIDE, (k + 1) * WIDE)
        i = R_MSG + 6 * k
        arrived(i, i + 1)
        cbuf[0, :, cols] = (
            r1buf[0, :, cols].astype(f32) + pbuf[xp, 0:32, cols].astype(f32)
        ).astype(bf16)
        cbuf[1, :, cols] = (
            r1buf[1, :, cols].astype(f32) + pbuf[xm, 32:64, cols].astype(f32)
        ).astype(bf16)
        start(i + 4, i + 5)
    for k in range(COLS):
        cols = slice(k * WIDE, (k + 1) * WIDE)
        i = R_MSG + 6 * k
        arrived(i + 2, i + 3, i + 4, i + 5)
        out[0:32, cols] = (
            pbuf[x, 0:32, cols].astype(f32)
            + crecv[0, :, cols].astype(f32)
            + dbuf[1, :, cols].astype(f32)
        ).astype(bf16)
        out[32:64, cols] = (
            pbuf[x, 32:64, cols].astype(f32)
            + crecv[1, :, cols].astype(f32)
            + dbuf[0, :, cols].astype(f32)
        ).astype(bf16)
    for i in range(N_MSG):
        send[i].wait_send()


def local(
    tokens,
    down_query,
    down_latent,
    down_rotary,
    query_gain,
    latent_gain,
    up_query,
    up_query_rotary,
    up_key,
    up_value,
    out_weight,
):
    sp = lax.axis_index("sp")
    x = lax.axis_index("tp")
    inverse = rope_base ** (-jnp.arange(0, ROPE, 2, dtype=f32) / ROPE)
    own = ((sp * RING + x) * OWN + jnp.arange(OWN, dtype=jnp.int32)).astype(f32)
    angles = own[:, None] * jnp.tile(inverse, 4)[None, :]
    sign = jnp.tile(jnp.repeat(jnp.array([-1.0, 1.0], f32), 32), 2)
    key_cos, key_sin = jnp.cos(angles), jnp.sin(angles) * sign[None, :]
    span = (sp * GROUP + jnp.arange(GROUP, dtype=jnp.int32)).astype(f32)
    angles = inverse[:, None] * span[None, :]
    query_cos, query_sin = jnp.cos(angles), jnp.sin(angles)

    vmem = pl.BlockSpec(memory_space=pltpu.VMEM)
    hbm = pl.BlockSpec(memory_space=pl.ANY)
    return pl.pallas_call(
        kernel,
        out_shape=jax.ShapeDtypeStruct((OWN, 4096), bf16),
        in_specs=[vmem, hbm, hbm, hbm, vmem, vmem, hbm, hbm, hbm, hbm, hbm, vmem, vmem, vmem, vmem],
        out_specs=vmem,
        scratch_shapes=[
            pltpu.VMEM((4096, 512), bf16),
            pltpu.VMEM((4096, 64), bf16),
            pltpu.VMEM((4096, 1024), bf16),
            pltpu.VMEM((1024, 512), bf16),
            pltpu.VMEM((1024, 256), bf16),
            pltpu.VMEM((512, 512), bf16),
            pltpu.VMEM((512, 512), bf16),
            pltpu.VMEM((512, 4096), bf16),
            pltpu.VMEM((16, 4, BLOCK, 128), bf16),
            pltpu.VMEM((4, OWN, 1024), bf16),
            pltpu.VMEM((2, HEADS * (NOPE + ROPE), GROUP), bf16),
            pltpu.VMEM((512, 512), bf16),
            pltpu.VMEM((HEADS, 2 * GROUP, 256), bf16),
            pltpu.VMEM((HEADS, VROWS, 2 * GROUP), bf16),
            pltpu.VMEM((2, HEADS, VROWS, GROUP), f32),
            pltpu.VMEM((2, HEADS, 1, GROUP), f32),
            pltpu.VMEM((HEADS, VROWS, GROUP), f32),
            pltpu.VMEM((HEADS, VROWS, GROUP), f32),
            pltpu.VMEM((4, OWN, 4096), bf16),
            pltpu.VMEM((2, 32, 4096), bf16),
            pltpu.VMEM((2, 32, 4096), bf16),
            pltpu.VMEM((2, 32, 4096), bf16),
            pltpu.VMEM((2, 32, 4096), bf16),
            pltpu.SemaphoreType.DMA((14,)),
            pltpu.SemaphoreType.DMA((N_MSG,)),
            pltpu.SemaphoreType.DMA((N_MSG,)),
        ],
        compiler_params=pltpu.CompilerParams(
            collective_id=0, has_side_effects=True, vmem_limit_bytes=62 * 1024 * 1024
        ),
    )(
        tokens,
        down_query,
        down_latent,
        down_rotary,
        query_gain.reshape(1, -1),
        latent_gain.reshape(1, -1),
        up_query,
        up_query_rotary,
        up_key,
        up_value,
        out_weight,
        key_cos,
        key_sin,
        query_cos,
        query_sin,
    )


def solution(mesh):
    return jax.shard_map(
        local,
        mesh=mesh,
        in_specs=(
            P(("sp", "tp"), None),
            P(),
            P(),
            P(),
            P(),
            P(),
            P(None, "tp"),
            P(None, "tp"),
            P(None, "tp"),
            P(None, "tp"),
            P("tp", None),
        ),
        out_specs=P(("sp", "tp"), None),
        check_vma=False,
    )
```

time: 239 us -> 87.2 us (0.36)
  the two profiles are of different devices: /device:TPU:96 before, /device:TPU:104 now
where the time goes in v1:
time: 87.2 us; the launch traced here: 87 us
  Pallas kernels  80 us (92%)
  local copies, waits for them, and re-layouts  5.22 us (6%)
  other arithmetic  1.67 us (2%)
    pallas_call x1, Pallas kernels, local(): pl.pallas_call(kernel, out_shape=jax.ShapeDtypeStruct((OWN, 4096), bf16),...  80 us
    unnamed x2, local copies, waits for them, and re-layouts  4.23 us

profile of v1, /device:TPU:104, one launch (start us, length us, event | category | flops | bytes accessed | tf_op | source)
XLA Modules:
  0.0 87.0 jit_solution(6078416365424313537)
XLA Ops:
  0.0 0.7 broadcast_in_dim.2
  0.8 0.1 tile.14
  0.8 0.1 mul.71
  0.9 0.1 mul.68
  1.0 0.8 fusion
  1.8 0.8 multiply_sine_fusion
  2.7 2.4 %copy.13.down_rotary = bf16[4096,64]{1,0:T(8,128)(2,1)} copy(bf16[4096,64]{0,1:T(8,128)(2,1)} %param.15) | data formatting | bytes 1048576 | tf_op args[3]
  5.0 80.0 %shard_map.118 = bf16[64,4096]{1,0:T(8,128)(2,1)} custom-call(bf16[64,4096]{1,0:T(8,128)(2,1)} %tokens.1, bf16[4096,1024]{1,0:T(8,128)(2,1)} %down_query.1, bf16[4096,512]{1,0:T(8,128)(2,1)} %down_latent.1, bf16[4096,64]{1,0:T(8,128)(2,1)} %copy.13.down_rotary, f32[1,1024]{1,0:T(1,128)} %bitcast.2, f32[1,512]{1,0:T(1,128)} %bitcast.3, ...), custom_call_target="tpu_custom_call" | custom-call | tf_op jit(solution)/shard_map/pallas_call | solution.py:459
  85.1 1.9 %copy.15 = bf16[64,4096]{1,0:T(8,128)(2,1)} copy(bf16[64,4096]{1,0:T(8,128)(2,1)} %shard_map.118) | data formatting | bytes 1048576
  (5 shorter events, 0.0 us)

commit v2 on v1

--- a/solution.py
+++ b/solution.py
@@ -77,6 +77,9 @@
     vbuf,
     acc,
     best,
+    qfull,
+    sbuf,
+    tops,
     xsend,
     xrecv,
     pbuf,
@@ -206,7 +209,9 @@
     for t in range(4):
         lat[s0, x, t * OWN : (t + 1) * OWN, :] = latent[:, t * 128 : (t + 1) * 128]
     loads[4].wait()
-    turned = jnp.dot(tokens[...], wdr[...], preferred_element_type=f32)
+    turned = lax.dot_general(
+        tokens[...], wdr[...], (((1,), (1,)), ((), ())), preferred_element_type=f32
+    )
     turned = jnp.concatenate([turned, turned], axis=-1)
     turned = turned * key_cos[...] + pltpu.roll(turned, 32, 1) * key_sin[...]
     lane = lax.broadcasted_iota(jnp.int32, (32, 128), 1)
@@ -251,6 +256,13 @@
         qt[c, at_row + 32 : at_row + 64, :] = (two * cosine + one * sine).astype(bf16)
     start(QX_MSG)
     arrived(QX_MSG)
+    for h in range(HEADS):
+        for j in range(2):
+            cols = slice(j * GROUP, (j + 1) * GROUP)
+            qfull[h, 0:NOPE, cols] = qt[j, h * NOPE : (h + 1) * NOPE, :]
+            at_row = HEADS * NOPE + h * ROPE
+            qfull[h, NOPE : NOPE + ROPE, cols] = qt[j, at_row : at_row + ROPE, :]
+        qfull[h, NOPE + ROPE :, :] = jnp.zeros((ROPE, 2 * GROUP), bf16)
 
     UNIT = 2 * GROUP
 
@@ -277,40 +289,29 @@
         for h in range(HEADS):
             vbuf[h, 0:VDIM, :] = values[h * VDIM : (h + 1) * VDIM]
 
-        def head(h, carry):
-            key = kbuf[h]
-            value = vbuf[h]
-            for j in range(2):
-                at_plain = pl.multiple_of(h * NOPE, NOPE)
-                at_turned = pl.multiple_of(HEADS * NOPE + h * ROPE, ROPE)
-                queries = jnp.concatenate(
-                    [
-                        qt[j, pl.ds(at_plain, NOPE), :],
-                        qt[j, pl.ds(at_turned, ROPE), :],
-                        jnp.zeros((ROPE, GROUP), bf16),
-                    ],
-                    axis=0,
-                )
-                scores = jnp.dot(key, queries, preferred_element_type=f32)
-                if masked:
-                    row = lax.broadcasted_iota(jnp.int32, (UNIT, GROUP), 0)
-                    col = lax.broadcasted_iota(jnp.int32, (UNIT, GROUP), 1)
-                    base_one = (2 * m_one + c) * GROUP
-                    base_two = (2 * m_two + c) * GROUP - GROUP
-                    place = row + jnp.where(row < GROUP, base_one, base_two)
-                    scores = jnp.where(
-                        place <= col + (2 * m + j) * GROUP, scores, masked_score
-                    )
-                old = best[j, h]
-                new = jnp.maximum(old, jnp.max(scores, axis=0, keepdims=True))
-                weights = jnp.exp2(scores - new).astype(bf16)
-                best[j, h] = new
-                acc[j, h] = acc[j, h] * jnp.exp2(old - new) + jnp.dot(
-                    value, weights, preferred_element_type=f32
-                )
-            return carry
-
-        lax.fori_loop(0, HEADS, head, 0)
+        def score(h):
+            scores = jnp.dot(kbuf[h], qfull[h], preferred_element_type=f32)
+            if masked:
+                row = lax.broadcasted_iota(jnp.int32, (UNIT, UNIT), 0)
+                col = lax.broadcasted_iota(jnp.int32, (UNIT, UNIT), 1)
+                base_one = (2 * m_one + c) * GROUP
+                base_two = (2 * m_two + c) * GROUP - GROUP
+                place = row + jnp.where(row < GROUP, base_one, base_two)
+                scores = jnp.where(place <= col + 2 * m * GROUP, scores, masked_score)
+            sbuf[h % 2] = scores
+            tops[h % 2] = jnp.max(scores, axis=0, keepdims=True)
+
+        score(0)
+        for h in range(HEADS):
+            if h + 1 < HEADS:
+                score(h + 1)
+            old = best[h]
+            new = jnp.maximum(old, tops[h % 2])
+            weights = jnp.exp2(sbuf[h % 2] - new).astype(bf16)
+            best[h] = new
+            acc[h] = acc[h] * jnp.exp2(old - new) + jnp.dot(
+                vbuf[h], weights, preferred_element_type=f32
+            )
 
     def unit(u, carry):
         @pl.when(u == 0)
@@ -365,19 +366,20 @@
 
     lax.fori_loop(0, 8, unit, 0)
 
-    other = 1 - c
+    mine_at = pl.ds(pl.multiple_of(c * GROUP, GROUP), GROUP)
+    other_at = pl.ds(pl.multiple_of((1 - c) * GROUP, GROUP), GROUP)
     for h in range(HEADS):
-        xsend[h, 0:136, :] = acc[other, h, 0:136, :]
-        xsend[h, 136:144, :] = jnp.broadcast_to(best[other, h], (8, GROUP))
+        xsend[h, 0:136, :] = acc[h, 0:136, other_at]
+        xsend[h, 136:144, :] = jnp.broadcast_to(best[h, :, other_at], (8, GROUP))
     start(OX_MSG)
     arrived(OX_MSG)
     heads = []
     for h in range(HEADS):
-        mine, theirs = best[c, h], xrecv[h, 136:137, :]
+        mine, theirs = best[h, :, mine_at], xrecv[h, 136:137, :]
         top = jnp.maximum(mine, theirs)
         w_mine, w_theirs = jnp.exp2(mine - top), jnp.exp2(theirs - top)
-        total = acc[c, h, 128:129, :] * w_mine + xrecv[h, 128:129, :] * w_theirs
-        summed = acc[c, h, 0:128, :] * w_mine + xrecv[h, 0:128, :] * w_theirs
+        total = acc[h, 128:129, mine_at] * w_mine + xrecv[h, 128:129, :] * w_theirs
+        summed = acc[h, 0:128, mine_at] * w_mine + xrecv[h, 0:128, :] * w_theirs
         heads.append(jnp.transpose(summed / total).astype(bf16))
     attended = jnp.concatenate(heads, axis=1)
 
@@ -463,7 +465,7 @@
         out_specs=vmem,
         scratch_shapes=[
             pltpu.VMEM((4096, 512), bf16),
-            pltpu.VMEM((4096, 64), bf16),
+            pltpu.VMEM((64, 4096), bf16),
             pltpu.VMEM((4096, 1024), bf16),
             pltpu.VMEM((1024, 512), bf16),
             pltpu.VMEM((1024, 256), bf16),
@@ -476,8 +478,11 @@
             pltpu.VMEM((512, 512), bf16),
             pltpu.VMEM((HEADS, 2 * GROUP, 256), bf16),
             pltpu.VMEM((HEADS, VROWS, 2 * GROUP), bf16),
-            pltpu.VMEM((2, HEADS, VROWS, GROUP), f32),
-            pltpu.VMEM((2, HEADS, 1, GROUP), f32),
+            pltpu.VMEM((HEADS, VROWS, 2 * GROUP), f32),
+            pltpu.VMEM((HEADS, 1, 2 * GROUP), f32),
+            pltpu.VMEM((HEADS, 256, 2 * GROUP), bf16),
+            pltpu.VMEM((2, 2 * GROUP, 2 * GROUP), f32),
+            pltpu.VMEM((2, 1, 2 * GROUP), f32),
             pltpu.VMEM((HEADS, VROWS, GROUP), f32),
             pltpu.VMEM((HEADS, VROWS, GROUP), f32),
             pltpu.VMEM((4, OWN, 4096), bf16),
@@ -496,7 +501,7 @@
         tokens,
         down_query,
         down_latent,
-        down_rotary,
+        down_rotary.T,
         query_gain.reshape(1, -1),
         latent_gain.reshape(1, -1),
         up_query,

time: 87.2 us -> 71.2 us (0.82)
  the two profiles are of different devices: /device:TPU:104 before, /device:TPU:96 now
where the time goes in v2:
time: 71.2 us; the launch traced here: 70.8 us
  Pallas kernels  66.3 us (93%)
  local copies, waits for them, and re-layouts  2.86 us (4%)
  other arithmetic  1.67 us (2%)
    pallas_call x1, Pallas kernels, local(): pl.pallas_call(kernel, out_shape=jax.ShapeDtypeStruct((OWN, 4096), bf16),...  66.3 us
    unnamed x1, local copies, waits for them, and re-layouts  1.87 us

profile of v2, /device:TPU:96, one launch (start us, length us, event | category | flops | bytes accessed | tf_op | source)
XLA Modules:
  0.0 70.8 jit_solution(3256910631658500126)
XLA Ops:
  0.0 0.7 %broadcast_in_dim.2 = f32[2,32]{1,0:T(2,128)S(1)} broadcast(f32[2]{0:T(128)} %constant.24.clone), dimensions={0} | broadcast | bytes 264 | tf_op jit(solution)/shard_map/broadcast_in_dim | solution.py:453
  0.8 0.1 tile.14
  0.8 0.1 mul.71
  0.9 0.1 mul.68
  1.0 0.8 %fusion = (f32[64,128]{1,0:T(8,128)}, f32[64,128]{1,0:T(8,128)}) fusion(f32[128]{0:T(128)S(1)} %mul.71, f32[128]{0:T(128)S(1)} %mul.68, f32[64]{0:T(128)S(1)} %add_convert_fusion.1), kind=kLoop, calls=%fused_computation.4 | loop fusion | flops 16384 | bytes 66816 | tf_op jit(solution)/shard_map/mul | solution.py:454
  1.8 0.8 %multiply_sine_fusion = (f32[32,256]{1,0:T(8,128)}, f32[32,256]{1,0:T(8,128)}) fusion(f32[256]{0:T(256)S(1)} %add_convert_fusion, f32[32]{0:T(128)S(1)} %multiply_power_fusion), kind=kLoop, calls=%fused_computation | loop fusion | flops 8192 | bytes 66688 | tf_op jit(solution)/shard_map/sin | solution.py:457
  2.7 66.3 %shard_map.118 = bf16[64,4096]{1,0:T(8,128)(2,1)} custom-call(bf16[64,4096]{1,0:T(8,128)(2,1)} %tokens.1, bf16[4096,1024]{1,0:T(8,128)(2,1)} %down_query.1, bf16[4096,512]{1,0:T(8,128)(2,1)} %down_latent.1, bf16[64,4096]{1,0:T(8,128)(2,1)} %bitcast.3, f32[1,1024]{1,0:T(1,128)} %bitcast.4, f32[1,512]{1,0:T(1,128)} %bitcast.5, bf16[1024,512]{1,0:T(8,128)(2,1)} %up_query.1, ...), custom_call_target="tpu_custom_call" | custom-call | tf_op jit(solution)/shard_map/pallas_call | solution.py:461
  69.0 1.9 %copy.14 = bf16[64,4096]{1,0:T(8,128)(2,1)} copy(bf16[64,4096]{1,0:T(8,128)(2,1)} %shard_map.118) | data formatting | bytes 1048576
  (5 shorter events, 0.0 us)

commit v3 on v2

v3 whole, which is shorter than its diff:
```python
import functools

import jax
import jax.numpy as jnp
import numpy as np
from jax import lax
from jax.experimental import pallas as pl
from jax.experimental.pallas import tpu as pltpu
from jax.sharding import PartitionSpec as P

NOPE = 128
ROPE = 64
VDIM = 128
HEADS = 4
OWN = 64
GROUP = 256
BLOCK = 288
VROWS = 144
RING = 4

rope_base = 500000.0
norm_eps = 1e-06
masked_score = -1e30

f32 = jnp.float32
bf16 = jnp.bfloat16
MESH = pl.DeviceIdType.MESH

COLS = 4
N_MSG = 104

UNIT_OA = ((0, -1, 2, 1, 0, -1, 1, -1), (1, 0, 0, 1, -1, 2, 2, 2))
UNIT_OB = ((0, 0, 0, 1, 2, -1, 2, 2), (0, 1, -1, -1, 1, 1, -1, 2))


def pick(index, values):
    out = jnp.int32(values[0])
    for i, v in enumerate(values[1:], 1):
        out = jnp.where(index == i, jnp.int32(v), out)
    return out


def mod4(v):
    return lax.rem(v + 8, 4)


def kernel(
    tokens_in,
    down_query,
    down_latent,
    down_rotary,
    query_gain,
    latent_gain,
    up_query,
    up_query_rotary,
    up_key,
    up_value,
    out_weight,
    lane_rates,
    row_rates,
    out,
    tokens,
    lrate,
    rrate,
    lgain,
    qgain,
    wdl,
    wdr,
    wdq,
    wuq,
    wur,
    wuk,
    wuv,
    wout,
    lat,
    ql,
    qt,
    uvt,
    kbuf,
    vbuf,
    acc,
    best,
    qfull,
    sbuf,
    tops,
    xsend,
    xrecv,
    pbuf,
    r1buf,
    dbuf,
    cbuf,
    crecv,
    local_sem,
    ssem,
    rsem,
):
    sp = lax.axis_index("sp")
    x = lax.axis_index("tp")
    c = lax.rem(sp, 2)
    m = sp // 2
    y = lax.rem(m, 4)
    z = m // 4
    first = c == 0
    a = jnp.where(first, y, z)
    b = jnp.where(first, z, y)
    stride_a = jnp.where(first, 2, 8)
    stride_b = jnp.where(first, 8, 2)

    def at(aa, bb):
        return {"sp": aa * stride_a + bb * stride_b + c, "tp": x}

    xp, xm, x2 = mod4(x + 1), mod4(x - 1), mod4(x + 2)
    dev_xp = {"sp": sp, "tp": xp}
    dev_xm = {"sp": sp, "tp": xm}
    dev_ap, dev_am = at(mod4(a + 1), b), at(mod4(a - 1), b)
    dev_bp, dev_bm = at(a, mod4(b + 1)), at(a, mod4(b - 1))
    dev_core = {"sp": sp + 1 - 2 * c, "tp": x}

    copies = []

    def copy_in(src, dst):
        copies.append(pltpu.make_async_copy(src, dst, local_sem.at[len(copies)]))
        copies[-1].start()
        return copies[-1]

    K4 = 1024
    quarters = [pl.ds(k * K4, K4) for k in range(4)]
    load_lanes = copy_in(lane_rates, lrate)
    load_tokens = copy_in(tokens_in, tokens)
    load_latent = [copy_in(down_latent.at[r], wdl.at[r]) for r in quarters]
    load_rotary = copy_in(down_rotary, wdr)
    load_rows = copy_in(row_rates, rrate)
    load_lgain = copy_in(latent_gain, lgain)
    load_qgain = copy_in(query_gain, qgain)
    load_query = [copy_in(down_query.at[r], wdq.at[r]) for r in quarters]
    load_rest = [
        copy_in(up_query, wuq),
        copy_in(up_query_rotary, wur),
        copy_in(up_key, wuk),
        copy_in(up_value, wuv),
        copy_in(out_weight, wout),
    ]

    barrier = pltpu.get_barrier_semaphore()
    for dev in (dev_xp, dev_xm, dev_ap, dev_am, dev_bp, dev_bm, dev_core):
        pl.semaphore_signal(barrier, inc=1, device_id=dev, device_id_type=MESH)

    send, recv = [], []

    def add(src, dst, landed, dev):
        i = len(send)
        for refs, done in ((src, dst), send), ((landed, landed), recv):
            done.append(
                pltpu.make_async_remote_copy(
                    src_ref=refs[0],
                    dst_ref=refs[1],
                    send_sem=ssem.at[i],
                    recv_sem=rsem.at[i],
                    device_id=dev,
                    device_id_type=MESH,
                )
            )
        return i

    def pair(up, up_landed, dev_up, down, down_landed, dev_down):
        return (
            add(lat.at[up], lat.at[up], lat.at[up_landed], dev_up),
            add(lat.at[down], lat.at[down], lat.at[down_landed], dev_down),
        )

    def group(oa, ob):
        return mod4(b + ob) * 4 + mod4(a + oa)

    def line(ob, start=0, count=4):
        return pl.ds(mod4(b + ob) * 4 + start, count)

    def xs(o):
        return mod4(x + o)

    OFFS = (0, 1, -1, 2)
    s0 = group(0, 0)
    every, pre, post = pl.ds(0, 4), pl.ds(0, 2), pl.ds(2, 2)
    early, late = pl.ds(48, 240), pl.ds(0, 48)
    late_lo, late_hi = pl.ds(0, 32), pl.ds(32, 16)
    lo, hi = pl.ds(0, BLOCK // 2), pl.ds(BLOCK // 2, BLOCK // 2)
    own_block = (s0, x)

    X1 = pair(own_block, (s0, xm), dev_xp, own_block, (s0, xp), dev_xm)
    X2 = pair((s0, xm, lo), (s0, x2, lo), dev_xp, (s0, xp, hi), (s0, x2, hi), dev_xm)
    A1, B1 = {}, {}
    for o in OFFS:
        block = (s0, xs(o), early)
        A1[o] = pair(
            block, (group(-1, 0), *block[1:]), dev_ap, block, (group(1, 0), *block[1:]), dev_am
        )
        B1[0, o] = pair(
            block, (group(0, -1), *block[1:]), dev_bp, block, (group(0, 1), *block[1:]), dev_bm
        )
    A2 = pair(
        (group(-1, 0), pre, early),
        (group(2, 0), pre, early),
        dev_ap,
        (group(1, 0), post, early),
        (group(2, 0), post, early),
        dev_am,
    )
    B2, PB1 = {}, {}
    for o in OFFS:
        whole = (group(o, 0), every, early)
        if o != 0:
            B1[o] = pair(
                whole, (group(o, -1), *whole[1:]), dev_bp, whole, (group(o, 1), *whole[1:]), dev_bm
            )
        B2[o] = pair(
            (group(o, -1), pre, early),
            (group(o, 2), pre, early),
            dev_bp,
            (group(o, 1), post, early),
            (group(o, 2), post, early),
            dev_bm,
        )
        part = (group(o, 0), x, late)
        PB1[o] = pair(
            part, (group(o, -1), x, late), dev_bp, part, (group(o, 1), x, late), dev_bm
        )
    part = (s0, x, late)
    PA1 = pair(part, (group(-1, 0), x, late), dev_ap, part, (group(1, 0), x, late), dev_am)
    PA2 = pair(
        (group(-1, 0), x, late_lo),
        (group(2, 0), x, late_lo),
        dev_ap,
        (group(1, 0), x, late_hi),
        (group(2, 0), x, late_hi),
        dev_am,
    )
    PB2 = pair(
        (line(-1, 0, 2), x, late),
        (line(2, 0, 2), x, late),
        dev_bp,
        (line(1, 2, 2), x, late),
        (line(2, 2, 2), x, late),
        dev_bm,
    )
    XL1, XL2, XP1, XP2 = {}, {}, {}, {}
    for o in (1, -1, 2):
        g = group(o, 0)
        XL1[o] = pair((g, x, late), (g, xm, late), dev_xp, (g, x, late), (g, xp, late), dev_xm)
        XL2[o] = pair(
            (g, xm, late_lo), (g, x2, late_lo), dev_xp, (g, xp, late_hi), (g, x2, late_hi), dev_xm
        )
        g = line(o)
        XP1[o] = pair((g, x, late), (g, xm, late), dev_xp, (g, x, late), (g, xp, late), dev_xm)
        g, h = line(o, 0, 2), line(o, 2, 2)
        XP2[o] = pair((g, xm, late), (g, x2, late), dev_xp, (h, xp, late), (h, x2, late), dev_xm)
    q_lo, q_hi = pl.ds(0, OWN // 2), pl.ds(OWN // 2, OWN // 2)
    Q1 = (
        add(ql.at[x], ql.at[x], ql.at[xm], dev_xp),
        add(ql.at[x], ql.at[x], ql.at[xp], dev_xm),
    )
    Q2 = (
        add(ql.at[xm, q_lo], ql.at[xm, q_lo], ql.at[x2, q_lo], dev_xp),
        add(ql.at[xp, q_hi], ql.at[xp, q_hi], ql.at[x2, q_hi], dev_xm),
    )
    QX = (add(qt.at[c], qt.at[c], qt.at[1 - c], dev_core),)
    OX = (add(xsend, xrecv, xrecv, dev_core),)

    def start(*groups):
        for ids in groups:
            for i in ids:
                send[i].start()

    def arrived(*groups):
        for ids in groups:
            for i in ids:
                recv[i].wait_recv()

    def norm_rows(values, gain):
        return values * lax.rsqrt(jnp.mean(values * values, axis=-1, keepdims=True) + norm_eps) * gain

    load_lanes.wait()
    spot = lax.broadcasted_iota(jnp.int32, (OWN, 128), 0) + (sp * RING + x) * OWN
    angles = spot.astype(f32) * lrate[...]
    lane = lax.broadcasted_iota(jnp.int32, (OWN, 128), 1)
    key_cos = jnp.cos(angles)
    key_sin = jnp.sin(angles) * jnp.where(lax.rem(lane, 64) < 32, -1.0, 1.0)
    load_tokens.wait()
    latent = jnp.zeros((OWN, 512), f32)
    for k in range(4):
        load_latent[k].wait()
        cols = slice(k * K4, (k + 1) * K4)
        latent = latent + jnp.dot(tokens[:, cols], wdl[cols, :], preferred_element_type=f32)
    load_lgain.wait()
    latent = norm_rows(latent, lgain[...]).astype(bf16)
    for t in range(4):
        lat[s0, x, t * OWN : (t + 1) * OWN, :] = latent[:, t * 128 : (t + 1) * 128]
    load_rotary.wait()
    turned = lax.dot_general(
        tokens[...], wdr[...], (((1,), (1,)), ((), ())), preferred_element_type=f32
    )
    turned = jnp.concatenate([turned, turned], axis=-1)
    turned = turned * key_cos + pltpu.roll(turned, 32, 1) * key_sin
    lat[s0, x, 256:288, :] = jnp.where(lane[:32] < 64, turned[:32], turned[32:]).astype(bf16)
    pl.semaphore_wait(barrier, 7)
    start(X1, PA1, B1[0, 0], A1[0], PB1[0])

    query = jnp.zeros((OWN, 1024), f32)
    for k in range(4):
        load_query[k].wait()
        cols = slice(k * K4, (k + 1) * K4)
        query = query + jnp.dot(tokens[:, cols], wdq[cols, :], preferred_element_type=f32)
    load_qgain.wait()
    ql[x] = norm_rows(query, qgain[...]).astype(bf16)
    start(Q1)
    arrived(PA1)
    start(PA2, XL1[1], XL1[-1], PB1[1], PB1[-1])
    load_rows.wait()
    for load in load_rest:
        load.wait()
    uvt[...] = jnp.transpose(wuv[...].astype(f32)).astype(bf16)
    for h in range(HEADS):
        vbuf[h, VDIM:VROWS, :] = jnp.ones((VROWS - VDIM, 2 * GROUP), bf16)
    acc[...] = jnp.zeros_like(acc)
    best[...] = jnp.full(best.shape, masked_score, f32)
    spot = lax.broadcasted_iota(jnp.int32, (32, GROUP), 1) + sp * GROUP
    angles = spot.astype(f32) * rrate[...]
    cosine, sine = jnp.cos(angles), jnp.sin(angles)
    arrived(X1)
    start(X2, A1[1], A1[-1], B1[0, 1], B1[0, -1])
    arrived(PA2)
    start(XL1[2], PB1[2])
    arrived(Q1)
    start(Q2)
    arrived(XL1[1], XL1[-1])
    start(XL2[1], XL2[-1])
    arrived(PB1[0], PB1[1], PB1[-1], PB1[2])
    start(PB2, XP1[1], XP1[-1])
    arrived(X2)
    start(A1[2], B1[0, 2])
    arrived(XL1[2])
    start(XL2[2])
    arrived(Q2)
    factor = (NOPE + ROPE) ** (-0.5) * 1.4426950408889634
    rows = ql[...].reshape(GROUP, 1024)
    plain = jnp.dot(rows, wuq[...], preferred_element_type=f32) * factor
    qt[c, 0 : HEADS * NOPE, :] = jnp.transpose(plain).astype(bf16)
    turned = jnp.transpose(jnp.dot(rows, wur[...], preferred_element_type=f32) * factor)
    for h in range(HEADS):
        one = turned[h * ROPE : h * ROPE + 32]
        two = turned[h * ROPE + 32 : (h + 1) * ROPE]
        at_row = HEADS * NOPE + h * ROPE
        qt[c, at_row : at_row + 32, :] = (one * cosine - two * sine).astype(bf16)
        qt[c, at_row + 32 : at_row + 64, :] = (two * cosine + one * sine).astype(bf16)
    start(QX)

    UNIT = 2 * GROUP

    def sets_of(u):
        sets, spots = [], []
        for n in range(2):
            aa = mod4(a + pick(u, UNIT_OA[n]))
            bb = mod4(b + pick(u, UNIT_OB[n]))
            sets.append(bb * 4 + aa)
            spots.append(jnp.where(first, bb * 4 + aa, aa * 4 + bb))
        return sets, spots

    def expand(u):
        parts, rots = [], []
        for s in sets_of(u)[0]:
            tiles = [
                lat[s, :, t * OWN : (t + 1) * OWN, :].reshape(GROUP, 128) for t in range(4)
            ]
            parts.append(jnp.concatenate(tiles, axis=1))
            packed = lat[s, :, 256:288, :]
            swapped = pltpu.roll(packed.reshape(128, 128).astype(f32), 64, 1).astype(bf16)
            rots.append(
                jnp.concatenate([packed, swapped.reshape(4, 32, 128)], axis=1).reshape(GROUP, 128)
            )
        latents = jnp.concatenate(parts, axis=0)
        kbuf[:, 0:512] = jnp.dot(latents, wuk[...], preferred_element_type=f32).astype(bf16)
        kbuf[:, 512:640] = jnp.concatenate(rots, axis=0)
        values = lax.dot_general(
            uvt[...], latents, (((1,), (1,)), ((), ())), preferred_element_type=f32
        ).astype(bf16)
        for h in range(HEADS):
            vbuf[h, 0:VDIM, :] = values[h * VDIM : (h + 1) * VDIM]

    def attend(spots, masked):
        def score(h):
            keys = jnp.concatenate(
                [kbuf[:, h * NOPE : (h + 1) * NOPE], kbuf[:, 512:640]], axis=1
            )
            scores = jnp.dot(keys, qfull[h], preferred_element_type=f32)
            if masked:
                row = lax.broadcasted_iota(jnp.int32, (UNIT, UNIT), 0)
                col = lax.broadcasted_iota(jnp.int32, (UNIT, UNIT), 1)
                base_one = (2 * spots[0] + c) * GROUP
                base_two = (2 * spots[1] + c) * GROUP - GROUP
                place = row + jnp.where(row < GROUP, base_one, base_two)
                scores = jnp.where(place <= col + 2 * m * GROUP, scores, masked_score)
            sbuf[h % 2] = scores
            tops[h % 2] = jnp.max(scores, axis=0, keepdims=True)

        score(0)
        for h in range(HEADS):
            if h + 1 < HEADS:
                score(h + 1)
            old = best[h]
            new = jnp.maximum(old, tops[h % 2])
            weights = jnp.exp2(sbuf[h % 2] - new).astype(bf16)
            best[h] = new
            acc[h] = acc[h] * jnp.exp2(old - new) + jnp.dot(
                vbuf[h], weights, preferred_element_type=f32
            )

    def needed(u):
        spots = sets_of(u)[1]
        return jnp.logical_or(spots[0] <= m, spots[1] <= m)

    arrived(PB2)
    start(XP1[2])
    arrived(A1[0], A1[1], A1[-1], A1[2])
    start(A2, B1[1], B1[-1])
    arrived(XL2[1], XL2[-1])

    def unit(u, carry):

        @pl.when(u == 1)
        def _():
            arrived(XP1[2])
            start(XP2[2])
            arrived(XP2[1], XP2[-1])

        @pl.when(u == 2)
        def _():
            arrived(A2)
            start(B1[2])
            arrived(XL2[2])

        @pl.when(u == 4)
        def _():
            arrived(B2[0], XP2[2])

        @pl.when(u == 5)
        def _():
            arrived(B1[2])
            start(B2[2])

        @pl.when(u == 6)
        def _():
            arrived(B2[1])

        @pl.when(u == 7)
        def _():
            arrived(B2[-1], B2[2])

        spots = sets_of(u)[1]
        plain_unit = jnp.logical_and(spots[0] < m, spots[1] < m)
        some = needed(u)

        @pl.when(some)
        def _():
            expand(u)


        @pl.when(u == 0)
        def _():
            arrived(B1[0, 0], B1[0, 1], B1[0, -1], B1[0, 2])
            start(B2[0])
            arrived(XP1[1], XP1[-1])
            start(XP2[1], XP2[-1])
            arrived(QX)
            for h in range(HEADS):
                for j in range(2):
                    cols = slice(j * GROUP, (j + 1) * GROUP)
                    qfull[h, 0:NOPE, cols] = qt[j, h * NOPE : (h + 1) * NOPE, :]
                    at_row = HEADS * NOPE + h * ROPE
                    qfull[h, NOPE : NOPE + ROPE, cols] = qt[j, at_row : at_row + ROPE, :]
                qfull[h, NOPE + ROPE :, :] = jnp.zeros((ROPE, 2 * GROUP), bf16)

        @pl.when(u == 2)
        def _():
            arrived(B1[1])
            start(B2[1])

        @pl.when(u == 3)
        def _():
            arrived(B1[-1])
            start(B2[-1])


        @pl.when(plain_unit)
        def _():
            attend(spots, False)

        @pl.when(jnp.logical_and(some, jnp.logical_not(plain_unit)))
        def _():
            attend(spots, True)

        return carry

    lax.fori_loop(0, 8, unit, 0)

    mine_at = pl.ds(pl.multiple_of(c * GROUP, GROUP), GROUP)
    other_at = pl.ds(pl.multiple_of((1 - c) * GROUP, GROUP), GROUP)
    for h in range(HEADS):
        xsend[h, 0:136, :] = acc[h, 0:136, other_at]
        xsend[h, 136:144, :] = jnp.broadcast_to(best[h, :, other_at], (8, GROUP))
    start(OX)
    arrived(OX)
    heads = []
    for h in range(HEADS):
        mine, theirs = best[h, :, mine_at], xrecv[h, 136:137, :]
        top = jnp.maximum(mine, theirs)
        w_mine, w_theirs = jnp.exp2(mine - top), jnp.exp2(theirs - top)
        total = acc[h, 128:129, mine_at] * w_mine + xrecv[h, 128:129, :] * w_theirs
        summed = acc[h, 0:128, mine_at] * w_mine + xrecv[h, 0:128, :] * w_theirs
        heads.append(jnp.transpose(summed / total).astype(bf16))
    attended = jnp.concatenate(heads, axis=1)

    WIDE = 4096 // COLS
    top, low = pl.ds(0, 32), pl.ds(32, 32)
    R1, RD, RC = [], [], []
    for k in range(COLS):
        cols = pl.ds(k * WIDE, WIDE)

        def both(to_up, to_down, ref):
            up, down = ref.at[0, :, cols], ref.at[1, :, cols]
            return add(to_up, up, up, dev_xp), add(to_down, down, down, dev_xm)

        R1.append(both(pbuf.at[x2, top, cols], pbuf.at[x2, low, cols], r1buf))
        RD.append(both(pbuf.at[xp, low, cols], pbuf.at[xm, top, cols], dbuf))
        RC.append(both(cbuf.at[0, :, cols], cbuf.at[1, :, cols], crecv))
    assert len(send) == N_MSG, len(send)
    for k in range(COLS):
        cols = slice(k * WIDE, (k + 1) * WIDE)
        part = jnp.dot(attended, wout[:, cols], preferred_element_type=f32).astype(bf16)
        pbuf[:, :, cols] = part.reshape(4, OWN, WIDE)
        start(R1[k])
    start(*RD)
    for k in range(COLS):
        cols = slice(k * WIDE, (k + 1) * WIDE)
        arrived(R1[k])
        cbuf[0, :, cols] = (
            r1buf[0, :, cols].astype(f32) + pbuf[xp, 0:32, cols].astype(f32)
        ).astype(bf16)
        cbuf[1, :, cols] = (
            r1buf[1, :, cols].astype(f32) + pbuf[xm, 32:64, cols].astype(f32)
        ).astype(bf16)
        start(RC[k])
    for k in range(COLS):
        cols = slice(k * WIDE, (k + 1) * WIDE)
        arrived(RD[k], RC[k])
        out[0:32, cols] = (
            pbuf[x, 0:32, cols].astype(f32)
            + crecv[0, :, cols].astype(f32)
            + dbuf[1, :, cols].astype(f32)
        ).astype(bf16)
        out[32:64, cols] = (
            pbuf[x, 32:64, cols].astype(f32)
            + crecv[1, :, cols].astype(f32)
            + dbuf[0, :, cols].astype(f32)
        ).astype(bf16)
    for i in range(N_MSG):
        send[i].wait_send()


def local(
    tokens,
    down_query,
    down_latent,
    down_rotary,
    query_gain,
    latent_gain,
    up_query,
    up_query_rotary,
    up_key,
    up_value,
    out_weight,
):
    rates = (rope_base ** (-np.arange(0, ROPE, 2) / ROPE)).astype(np.float32)
    lane_rates = jnp.asarray(np.tile(rates, 4)[None, :])
    row_rates = jnp.asarray(np.repeat(rates[:, None], GROUP, axis=1))
    vmem = pl.BlockSpec(memory_space=pltpu.VMEM)
    hbm = pl.BlockSpec(memory_space=pl.ANY)
    return pl.pallas_call(
        kernel,
        out_shape=pltpu.VMEM((OWN, 4096), bf16),
        in_specs=[hbm] * 13,
        out_specs=vmem,
        scratch_shapes=[
            pltpu.VMEM((OWN, 4096), bf16),
            pltpu.VMEM((1, 128), f32),
            pltpu.VMEM((32, GROUP), f32),
            pltpu.VMEM((1, 512), f32),
            pltpu.VMEM((1, 1024), f32),
            pltpu.VMEM((4096, 512), bf16),
            pltpu.VMEM((64, 4096), bf16),
            pltpu.VMEM((4096, 1024), bf16),
            pltpu.VMEM((1024, 512), bf16),
            pltpu.VMEM((1024, 256), bf16),
            pltpu.VMEM((512, 512), bf16),
            pltpu.VMEM((512, 512), bf16),
            pltpu.VMEM((512, 4096), bf16),
            pltpu.VMEM((16, 4, BLOCK, 128), bf16),
            pltpu.VMEM((4, OWN, 1024), bf16),
            pltpu.VMEM((2, HEADS * (NOPE + ROPE), GROUP), bf16),
            pltpu.VMEM((512, 512), bf16),
            pltpu.VMEM((2 * GROUP, 640), bf16),
            pltpu.VMEM((HEADS, VROWS, 2 * GROUP), bf16),
            pltpu.VMEM((HEADS, VROWS, 2 * GROUP), f32),
            pltpu.VMEM((HEADS, 1, 2 * GROUP), f32),
            pltpu.VMEM((HEADS, 256, 2 * GROUP), bf16),
            pltpu.VMEM((2, 2 * GROUP, 2 * GROUP), f32),
            pltpu.VMEM((2, 1, 2 * GROUP), f32),
            pltpu.VMEM((HEADS, VROWS, GROUP), f32),
            pltpu.VMEM((HEADS, VROWS, GROUP), f32),
            pltpu.VMEM((4, OWN, 4096), bf16),
            pltpu.VMEM((2, 32, 4096), bf16),
            pltpu.VMEM((2, 32, 4096), bf16),
            pltpu.VMEM((2, 32, 4096), bf16),
            pltpu.VMEM((2, 32, 4096), bf16),
            pltpu.SemaphoreType.DMA((19,)),
            pltpu.SemaphoreType.DMA((N_MSG,)),
            pltpu.SemaphoreType.DMA((N_MSG,)),
        ],
        compiler_params=pltpu.CompilerParams(
            collective_id=0, has_side_effects=True, vmem_limit_bytes=62 * 1024 * 1024
        ),
    )(
        tokens,
        down_query,
        down_latent,
        down_rotary.T,
        query_gain.reshape(1, -1),
        latent_gain.reshape(1, -1),
        up_query,
        up_query_rotary,
        up_key,
        up_value,
        out_weight,
        lane_rates,
        row_rates,
    )


def solution(mesh):
    return jax.shard_map(
        local,
        mesh=mesh,
        in_specs=(
            P(("sp", "tp"), None),
            P(),
            P(),
            P(),
            P(),
            P(),
            P(None, "tp"),
            P(None, "tp"),
            P(None, "tp"),
            P(None, "tp"),
            P("tp", None),
        ),
        out_specs=P(("sp", "tp"), None),
        check_vma=False,
    )
```

time: 71.2 us -> 64.4 us (0.904)
  the two profiles are of different devices: /device:TPU:96 before, /device:TPU:1 now
where the time goes in v3:
time: 64.4 us; the launch traced here: 64.3 us
  Pallas kernels  63.5 us (99%)
  local copies, waits for them, and re-layouts  0.8 us (1%)
    pallas_call x1, Pallas kernels, local(): pl.pallas_call(kernel, out_shape=pltpu.VMEM((OWN, 4096), bf16), in_specs=...  63.5 us

profile of v3, /device:TPU:1, one launch (start us, length us, event | category | flops | bytes accessed | tf_op | source)
XLA Modules:
  0.0 64.3 jit_solution(12593519335337860442)
XLA Ops:
  0.0 63.5 %shard_map.127 = bf16[64,4096]{1,0:T(8,128)(2,1)S(1)} custom-call(bf16[64,4096]{1,0:T(8,128)(2,1)} %tokens_in.1, bf16[4096,1024]{1,0:T(8,128)(2,1)} %down_query.1, bf16[4096,512]{1,0:T(8,128)(2,1)} %down_latent.1, bf16[64,4096]{1,0:T(8,128)(2,1)} %bitcast.3, f32[1,1024]{1,0:T(1,128)} %bitcast.4, f32[1,512]{1,0:T(1,128)} %bitcast.5, ...), custom_call_target="tpu_custom_call" | custom-call | tf_op jit(solution)/shard_map/pallas_call | solution.py:585
  63.5 0.8 %copy.15 = bf16[64,4096]{1,0:T(8,128)(2,1)} copy(bf16[64,4096]{1,0:T(8,128)(2,1)S(1)} %shard_map.127) | data formatting | bytes 1048576

commit v4 on v3

--- a/solution.py
+++ b/solution.py
@@ -27,10 +27,11 @@
 MESH = pl.DeviceIdType.MESH
 
 COLS = 4
-N_MSG = 104
-
-UNIT_OA = ((0, -1, 2, 1, 0, -1, 1, -1), (1, 0, 0, 1, -1, 2, 2, 2))
-UNIT_OB = ((0, 0, 0, 1, 2, -1, 2, 2), (0, 1, -1, -1, 1, 1, -1, 2))
+N_MSG = 102 + 6 * (COLS - 4)
+
+STEPS = 9
+UNIT_OA = ((0, 1, 0, 2, 1, -1, 2, 1, 2), (0, -1, 0, 1, -1, 0, 2, -1, 2))
+UNIT_OB = ((0, 0, 1, 0, -1, -1, 1, 2, 2), (0, 0, -1, 1, 1, 2, -1, 2, 2))
 
 
 def pick(index, values):
@@ -40,8 +41,19 @@
     return out
 
 
+def once(condition):
+    def run(body):
+        def trip(_, carry):
+            body()
+            return carry
+
+        lax.fori_loop(0, jnp.where(condition, 1, 0), trip, 0)
+
+    return run
+
+
 def mod4(v):
-    return lax.rem(v + 8, 4)
+    return jnp.where(v < 0, v + 4, jnp.where(v > 3, v - 4, v))
 
 
 def kernel(
@@ -85,6 +97,8 @@
     tops,
     xsend,
     xrecv,
+    ssend,
+    srecv,
     pbuf,
     r1buf,
     dbuf,
@@ -171,98 +185,58 @@
     def group(oa, ob):
         return mod4(b + ob) * 4 + mod4(a + oa)
 
-    def line(ob, start=0, count=4):
-        return pl.ds(mod4(b + ob) * 4 + start, count)
-
     def xs(o):
         return mod4(x + o)
 
     OFFS = (0, 1, -1, 2)
     s0 = group(0, 0)
-    every, pre, post = pl.ds(0, 4), pl.ds(0, 2), pl.ds(2, 2)
-    early, late = pl.ds(48, 240), pl.ds(0, 48)
-    late_lo, late_hi = pl.ds(0, 32), pl.ds(32, 16)
     lo, hi = pl.ds(0, BLOCK // 2), pl.ds(BLOCK // 2, BLOCK // 2)
-    own_block = (s0, x)
-
-    X1 = pair(own_block, (s0, xm), dev_xp, own_block, (s0, xp), dev_xm)
+
+    def block(oa, ob, o):
+        return group(oa, ob), xs(o)
+
+    X1 = [
+        pair((s0, x, up), (s0, xm, up), dev_xp, (s0, x, down), (s0, xp, down), dev_xm)
+        for up, down in ((lo, hi), (hi, lo))
+    ]
     X2 = pair((s0, xm, lo), (s0, x2, lo), dev_xp, (s0, xp, hi), (s0, x2, hi), dev_xm)
-    A1, B1 = {}, {}
+    A1, A2, B1, B2 = {}, {}, {}, {}
     for o in OFFS:
-        block = (s0, xs(o), early)
         A1[o] = pair(
-            block, (group(-1, 0), *block[1:]), dev_ap, block, (group(1, 0), *block[1:]), dev_am
+            block(0, 0, o), block(-1, 0, o), dev_ap, block(0, 0, o), block(1, 0, o), dev_am
         )
-        B1[0, o] = pair(
-            block, (group(0, -1), *block[1:]), dev_bp, block, (group(0, 1), *block[1:]), dev_bm
+        for oa in OFFS:
+            B1[oa, o] = pair(
+                block(oa, 0, o), block(oa, -1, o), dev_bp, block(oa, 0, o), block(oa, 1, o), dev_bm
+            )
+    for n, (up, down) in enumerate(((0, 1), (2, -1))):
+        A2[n] = pair(
+            block(-1, 0, up), block(2, 0, up), dev_ap, block(1, 0, down), block(2, 0, down), dev_am
         )
-    A2 = pair(
-        (group(-1, 0), pre, early),
-        (group(2, 0), pre, early),
-        dev_ap,
-        (group(1, 0), post, early),
-        (group(2, 0), post, early),
-        dev_am,
-    )
-    B2, PB1 = {}, {}
-    for o in OFFS:
-        whole = (group(o, 0), every, early)
-        if o != 0:
-            B1[o] = pair(
-                whole, (group(o, -1), *whole[1:]), dev_bp, whole, (group(o, 1), *whole[1:]), dev_bm
+        for oa in OFFS:
+            B2[oa, n] = pair(
+                block(oa, -1, up),
+                block(oa, 2, up),
+                dev_bp,
+                block(oa, 1, down),
+                block(oa, 2, down),
+                dev_bm,
             )
-        B2[o] = pair(
-            (group(o, -1), pre, early),
-            (group(o, 2), pre, early),
-            dev_bp,
-            (group(o, 1), post, early),
-            (group(o, 2), post, early),
-            dev_bm,
+    q_lo, q_hi = pl.ds(0, OWN // 2), pl.ds(OWN // 2, OWN // 2)
+    Q1 = [
+        (
+            add(ql.at[x, up], ql.at[x, up], ql.at[xm, up], dev_xp),
+            add(ql.at[x, down], ql.at[x, down], ql.at[xp, down], dev_xm),
         )
-        part = (group(o, 0), x, late)
-        PB1[o] = pair(
-            part, (group(o, -1), x, late), dev_bp, part, (group(o, 1), x, late), dev_bm
-        )
-    part = (s0, x, late)
-    PA1 = pair(part, (group(-1, 0), x, late), dev_ap, part, (group(1, 0), x, late), dev_am)
-    PA2 = pair(
-        (group(-1, 0), x, late_lo),
-        (group(2, 0), x, late_lo),
-        dev_ap,
-        (group(1, 0), x, late_hi),
-        (group(2, 0), x, late_hi),
-        dev_am,
-    )
-    PB2 = pair(
-        (line(-1, 0, 2), x, late),
-        (line(2, 0, 2), x, late),
-        dev_bp,
-        (line(1, 2, 2), x, late),
-        (line(2, 2, 2), x, late),
-        dev_bm,
-    )
-    XL1, XL2, XP1, XP2 = {}, {}, {}, {}
-    for o in (1, -1, 2):
-        g = group(o, 0)
-        XL1[o] = pair((g, x, late), (g, xm, late), dev_xp, (g, x, late), (g, xp, late), dev_xm)
-        XL2[o] = pair(
-            (g, xm, late_lo), (g, x2, late_lo), dev_xp, (g, xp, late_hi), (g, x2, late_hi), dev_xm
-        )
-        g = line(o)
-        XP1[o] = pair((g, x, late), (g, xm, late), dev_xp, (g, x, late), (g, xp, late), dev_xm)
-        g, h = line(o, 0, 2), line(o, 2, 2)
-        XP2[o] = pair((g, xm, late), (g, x2, late), dev_xp, (h, xp, late), (h, x2, late), dev_xm)
-    q_lo, q_hi = pl.ds(0, OWN // 2), pl.ds(OWN // 2, OWN // 2)
-    Q1 = (
-        add(ql.at[x], ql.at[x], ql.at[xm], dev_xp),
-        add(ql.at[x], ql.at[x], ql.at[xp], dev_xm),
-    )
+        for up, down in ((q_lo, q_hi), (q_hi, q_lo))
+    ]
     Q2 = (
         add(ql.at[xm, q_lo], ql.at[xm, q_lo], ql.at[x2, q_lo], dev_xp),
         add(ql.at[xp, q_hi], ql.at[xp, q_hi], ql.at[x2, q_hi], dev_xm),
     )
     QX = (add(qt.at[c], qt.at[c], qt.at[1 - c], dev_core),)
-    OX = (add(xsend, xrecv, xrecv, dev_core),)
+    OX = [(add(xsend.at[h], xrecv.at[h], xrecv.at[h], dev_core),) for h in range(HEADS)]
+    OS = (add(ssend, srecv, srecv, dev_core),)
 
     def start(*groups):
         for ids in groups:
@@ -301,7 +275,7 @@
     turned = turned * key_cos + pltpu.roll(turned, 32, 1) * key_sin
     lat[s0, x, 256:288, :] = jnp.where(lane[:32] < 64, turned[:32], turned[32:]).astype(bf16)
     pl.semaphore_wait(barrier, 7)
-    start(X1, PA1, B1[0, 0], A1[0], PB1[0])
+    start(*X1, A1[0], B1[0, 0])
 
     query = jnp.zeros((OWN, 1024), f32)
     for k in range(4):
@@ -310,9 +284,11 @@
         query = query + jnp.dot(tokens[:, cols], wdq[cols, :], preferred_element_type=f32)
     load_qgain.wait()
     ql[x] = norm_rows(query, qgain[...]).astype(bf16)
-    start(Q1)
-    arrived(PA1)
-    start(PA2, XL1[1], XL1[-1], PB1[1], PB1[-1])
+    start(*Q1)
+    arrived(X1[0])
+    start(X2)
+    arrived(X1[1])
+    start(A1[1], A1[-1], B1[0, 1], B1[0, -1])
     load_rows.wait()
     for load in load_rest:
         load.wait()
@@ -324,21 +300,19 @@
     spot = lax.broadcasted_iota(jnp.int32, (32, GROUP), 1) + sp * GROUP
     angles = spot.astype(f32) * rrate[...]
     cosine, sine = jnp.cos(angles), jnp.sin(angles)
-    arrived(X1)
-    start(X2, A1[1], A1[-1], B1[0, 1], B1[0, -1])
-    arrived(PA2)
-    start(XL1[2], PB1[2])
-    arrived(Q1)
+    arrived(A1[0])
+    start(B1[1, 0], B1[-1, 0])
+    arrived(Q1[0])
     start(Q2)
-    arrived(XL1[1], XL1[-1])
-    start(XL2[1], XL2[-1])
-    arrived(PB1[0], PB1[1], PB1[-1], PB1[2])
-    start(PB2, XP1[1], XP1[-1])
+    arrived(A1[1])
+    start(A2[0], B1[1, 1], B1[-1, 1])
+    arrived(B1[0, 0], B1[0, 1])
+    start(B2[0, 0])
     arrived(X2)
     start(A1[2], B1[0, 2])
-    arrived(XL1[2])
-    start(XL2[2])
-    arrived(Q2)
+    arrived(A1[-1])
+    start(B1[1, -1], B1[-1, -1])
+    arrived(Q1[1], Q2)
     factor = (NOPE + ROPE) ** (-0.5) * 1.4426950408889634
     rows = ql[...].reshape(GROUP, 1024)
     plain = jnp.dot(rows, wuq[...], preferred_element_type=f32) * factor
@@ -352,20 +326,18 @@
         qt[c, at_row + 32 : at_row + 64, :] = (two * cosine + one * sine).astype(bf16)
     start(QX)
 
-    UNIT = 2 * GROUP
-
-    def sets_of(u):
-        sets, spots = [], []
-        for n in range(2):
-            aa = mod4(a + pick(u, UNIT_OA[n]))
-            bb = mod4(b + pick(u, UNIT_OB[n]))
-            sets.append(bb * 4 + aa)
-            spots.append(jnp.where(first, bb * 4 + aa, aa * 4 + bb))
-        return sets, spots
-
-    def expand(u):
+    def set_of(u, n):
+        aa, bb = mod4(a + pick(u, UNIT_OA[n])), mod4(b + pick(u, UNIT_OB[n]))
+        spot = jnp.where(first, bb * 4 + aa, aa * 4 + bb)
+        seen = spot <= m
+        if n == 1:
+            seen = jnp.logical_and(seen, jnp.logical_and(u > 0, u < STEPS - 1))
+        return bb * 4 + aa, spot, seen
+
+    def expand(sets):
+        keys = len(sets) * GROUP
         parts, rots = [], []
-        for s in sets_of(u)[0]:
+        for s in sets:
             tiles = [
                 lat[s, :, t * OWN : (t + 1) * OWN, :].reshape(GROUP, 128) for t in range(4)
             ]
@@ -376,28 +348,26 @@
                 jnp.concatenate([packed, swapped.reshape(4, 32, 128)], axis=1).reshape(GROUP, 128)
             )
         latents = jnp.concatenate(parts, axis=0)
-        kbuf[:, 0:512] = jnp.dot(latents, wuk[...], preferred_element_type=f32).astype(bf16)
-        kbuf[:, 512:640] = jnp.concatenate(rots, axis=0)
+        kbuf[:keys, 0:512] = jnp.dot(latents, wuk[...], preferred_element_type=f32).astype(bf16)
+        kbuf[:keys, 512:640] = jnp.concatenate(rots, axis=0)
         values = lax.dot_general(
             uvt[...], latents, (((1,), (1,)), ((), ())), preferred_element_type=f32
         ).astype(bf16)
         for h in range(HEADS):
-            vbuf[h, 0:VDIM, :] = values[h * VDIM : (h + 1) * VDIM]
-
-    def attend(spots, masked):
+            vbuf[h, 0:VDIM, :keys] = values[h * VDIM : (h + 1) * VDIM]
+
+    def attend(keys, spot):
         def score(h):
-            keys = jnp.concatenate(
-                [kbuf[:, h * NOPE : (h + 1) * NOPE], kbuf[:, 512:640]], axis=1
+            key = jnp.concatenate(
+                [kbuf[:keys, h * NOPE : (h + 1) * NOPE], kbuf[:keys, 512:640]], axis=1
             )
-            scores = jnp.dot(keys, qfull[h], preferred_element_type=f32)
-            if masked:
-                row = lax.broadcasted_iota(jnp.int32, (UNIT, UNIT), 0)
-                col = lax.broadcasted_iota(jnp.int32, (UNIT, UNIT), 1)
-                base_one = (2 * spots[0] + c) * GROUP
-                base_two = (2 * spots[1] + c) * GROUP - GROUP
-                place = row + jnp.where(row < GROUP, base_one, base_two)
-                scores = jnp.where(place <= col + 2 * m * GROUP, scores, masked_score)
-            sbuf[h % 2] = scores
+            scores = jnp.dot(key, qfull[h], preferred_element_type=f32)
+            if spot is not None:
+                row = lax.broadcasted_iota(jnp.int32, (keys, 2 * GROUP), 0)
+                col = lax.broadcasted_iota(jnp.int32, (keys, 2 * GROUP), 1)
+                ahead = (2 * (spot - m) + c) * GROUP
+                scores = jnp.where(row + ahead <= col, scores, masked_score)
+            sbuf[h % 2, :keys] = scores
             tops[h % 2] = jnp.max(scores, axis=0, keepdims=True)
 
         score(0)
@@ -406,68 +376,72 @@
                 score(h + 1)
             old = best[h]
             new = jnp.maximum(old, tops[h % 2])
-            weights = jnp.exp2(sbuf[h % 2] - new).astype(bf16)
+            weights = jnp.exp2(sbuf[h % 2, :keys] - new).astype(bf16)
             best[h] = new
             acc[h] = acc[h] * jnp.exp2(old - new) + jnp.dot(
-                vbuf[h], weights, preferred_element_type=f32
+                vbuf[h, :, :keys], weights, preferred_element_type=f32
             )
 
-    def needed(u):
-        spots = sets_of(u)[1]
-        return jnp.logical_or(spots[0] <= m, spots[1] <= m)
-
-    arrived(PB2)
-    start(XP1[2])
-    arrived(A1[0], A1[1], A1[-1], A1[2])
-    start(A2, B1[1], B1[-1])
-    arrived(XL2[1], XL2[-1])
-
-    def unit(u, carry):
-
-        @pl.when(u == 1)
-        def _():
-            arrived(XP1[2])
-            start(XP2[2])
-            arrived(XP2[1], XP2[-1])
-
-        @pl.when(u == 2)
-        def _():
-            arrived(A2)
-            start(B1[2])
-            arrived(XL2[2])
-
-        @pl.when(u == 4)
-        def _():
-            arrived(B2[0], XP2[2])
-
-        @pl.when(u == 5)
-        def _():
-            arrived(B1[2])
-            start(B2[2])
-
-        @pl.when(u == 6)
-        def _():
-            arrived(B2[1])
-
-        @pl.when(u == 7)
-        def _():
-            arrived(B2[-1], B2[2])
-
-        spots = sets_of(u)[1]
-        plain_unit = jnp.logical_and(spots[0] < m, spots[1] < m)
-        some = needed(u)
-
-        @pl.when(some)
-        def _():
-            expand(u)
-
-
-        @pl.when(u == 0)
-        def _():
-            arrived(B1[0, 0], B1[0, 1], B1[0, -1], B1[0, 2])
-            start(B2[0])
-            arrived(XP1[1], XP1[-1])
-            start(XP2[1], XP2[-1])
+    arrived(A2[0])
+    start(B1[2, 0], B1[2, 1])
+    arrived(B1[1, 0], B1[1, 1])
+    start(B2[1, 0])
+    def far_seen(oa):
+        aa, bb = mod4(a + oa), mod4(b + 2)
+        return jnp.where(first, bb * 4 + aa, aa * 4 + bb) <= m
+
+    def step(u, carry):
+
+        @once(u == 1)
+        def _():
+            arrived(A1[2])
+            start(A2[1], B1[1, 2], B1[-1, 2])
+            arrived(B1[-1, 0], B1[-1, 1])
+            start(B2[-1, 0])
+
+        @once(u == 2)
+        def _():
+            arrived(B1[0, -1], B1[0, 2])
+            start(B2[0, 1])
+
+        @once(u == 3)
+        def _():
+            arrived(A2[1])
+            start(B1[2, -1], B1[2, 2])
+            arrived(B1[1, -1], B1[1, 2])
+            start(B2[1, 1])
+
+        @once(u == 4)
+        def _():
+            arrived(B1[2, 0], B1[2, 1])
+            start(B2[2, 0])
+            arrived(B1[-1, -1], B1[-1, 2])
+            start(B2[-1, 1])
+
+        for oa, when in ((0, 5), (1, 7), (-1, 7), (2, 8)):
+
+            @once(jnp.logical_and(u == when, far_seen(oa)))
+            def _(oa=oa):
+                arrived(B2[oa, 0], B2[oa, 1])
+
+        set_one, spot_one, seen_one = set_of(u, 0)
+        set_two, spot_two, seen_two = set_of(u, 1)
+        two = jnp.logical_and(seen_one, seen_two)
+        one = jnp.logical_and(jnp.logical_or(seen_one, seen_two), jnp.logical_not(two))
+        single = jnp.where(seen_one, set_one, set_two)
+        spot = jnp.where(seen_one, spot_one, spot_two)
+
+        @pl.when(two)
+        def _():
+            expand((set_one, set_two))
+
+        @pl.when(one)
+        def _():
+            expand((single,))
+
+
+        @once(u == 0)
+        def _():
             arrived(QX)
             for h in range(HEADS):
                 for j in range(2):
@@ -477,43 +451,42 @@
                     qfull[h, NOPE : NOPE + ROPE, cols] = qt[j, at_row : at_row + ROPE, :]
                 qfull[h, NOPE + ROPE :, :] = jnp.zeros((ROPE, 2 * GROUP), bf16)
 
-        @pl.when(u == 2)
-        def _():
-            arrived(B1[1])
-            start(B2[1])
-
-        @pl.when(u == 3)
-        def _():
-            arrived(B1[-1])
-            start(B2[-1])
-
-
-        @pl.when(plain_unit)
-        def _():
-            attend(spots, False)
-
-        @pl.when(jnp.logical_and(some, jnp.logical_not(plain_unit)))
-        def _():
-            attend(spots, True)
+        @once(u == 5)
+        def _():
+            arrived(B1[2, -1], B1[2, 2])
+            start(B2[2, 1])
+
+
+        @pl.when(two)
+        def _():
+            attend(2 * GROUP, None)
+
+        @pl.when(one)
+        def _():
+            attend(GROUP, spot)
 
         return carry
 
-    lax.fori_loop(0, 8, unit, 0)
+    lax.fori_loop(0, STEPS, step, 0)
 
     mine_at = pl.ds(pl.multiple_of(c * GROUP, GROUP), GROUP)
     other_at = pl.ds(pl.multiple_of((1 - c) * GROUP, GROUP), GROUP)
     for h in range(HEADS):
-        xsend[h, 0:136, :] = acc[h, 0:136, other_at]
-        xsend[h, 136:144, :] = jnp.broadcast_to(best[h, :, other_at], (8, GROUP))
-    start(OX)
-    arrived(OX)
+        ssend[h, 0:1, :] = best[h, :, other_at]
+        ssend[h, 1:2, :] = acc[h, 128:129, other_at]
+    start(OS)
+    for h in range(HEADS):
+        xsend[h] = acc[h, 0:128, other_at].astype(bf16)
+        start(OX[h])
+    arrived(OS)
     heads = []
     for h in range(HEADS):
-        mine, theirs = best[h, :, mine_at], xrecv[h, 136:137, :]
+        mine, theirs = best[h, :, mine_at], srecv[h, 0:1, :]
         top = jnp.maximum(mine, theirs)
         w_mine, w_theirs = jnp.exp2(mine - top), jnp.exp2(theirs - top)
-        total = acc[h, 128:129, mine_at] * w_mine + xrecv[h, 128:129, :] * w_theirs
-        summed = acc[h, 0:128, mine_at] * w_mine + xrecv[h, 0:128, :] * w_theirs
+        total = acc[h, 128:129, mine_at] * w_mine + srecv[h, 1:2, :] * w_theirs
+        arrived(OX[h])
+        summed = acc[h, 0:128, mine_at] * w_mine + xrecv[h].astype(f32) * w_theirs
         heads.append(jnp.transpose(summed / total).astype(bf16))
     attended = jnp.concatenate(heads, axis=1)
 
@@ -560,6 +533,12 @@
             + crecv[1, :, cols].astype(f32)
             + dbuf[0, :, cols].astype(f32)
         ).astype(bf16)
+    for oa in OFFS:
+
+        @pl.when(jnp.logical_not(far_seen(oa)))
+        def _(oa=oa):
+            arrived(B2[oa, 0], B2[oa, 1])
+
     for i in range(N_MSG):
         send[i].wait_send()
 
@@ -612,8 +591,10 @@
             pltpu.VMEM((HEADS, 256, 2 * GROUP), bf16),
             pltpu.VMEM((2, 2 * GROUP, 2 * GROUP), f32),
             pltpu.VMEM((2, 1, 2 * GROUP), f32),
-            pltpu.VMEM((HEADS, VROWS, GROUP), f32),
-            pltpu.VMEM((HEADS, VROWS, GROUP), f32),
+            pltpu.VMEM((HEADS, VDIM, GROUP), bf16),
+            pltpu.VMEM((HEADS, VDIM, GROUP), bf16),
+            pltpu.VMEM((HEADS, 8, GROUP), f32),
+            pltpu.VMEM((HEADS, 8, GROUP), f32),
             pltpu.VMEM((4, OWN, 4096), bf16),
             pltpu.VMEM((2, 32, 4096), bf16),
             pltpu.VMEM((2, 32, 4096), bf16),

time: 64.4 us -> 61.3 us (0.952)
  the two profiles are of different devices: /device:TPU:1 before, /device:TPU:96 now
where the time goes in v4:
time: 61.3 us; the launch traced here: 61.2 us
  Pallas kernels  60.4 us (99%)
  local copies, waits for them, and re-layouts  0.8 us (1%)
    pallas_call x1, Pallas kernels, local(): pl.pallas_call(kernel, out_shape=pltpu.VMEM((OWN, 4096), bf16), in_specs=...  60.4 us

profile of v4, /device:TPU:96, one launch (start us, length us, event | category | flops | bytes accessed | tf_op | source)
XLA Modules:
  0.0 61.2 jit_solution(1592479303456472956)
XLA Ops:
  0.0 60.4 %shard_map.127 = bf16[64,4096]{1,0:T(8,128)(2,1)S(1)} custom-call(bf16[64,4096]{1,0:T(8,128)(2,1)} %tokens_in.1, bf16[4096,1024]{1,0:T(8,128)(2,1)} %down_query.1, bf16[4096,512]{1,0:T(8,128)(2,1)} %down_latent.1, bf16[64,4096]{1,0:T(8,128)(2,1)} %bitcast.3, f32[1,1024]{1,0:T(1,128)} %bitcast.4, f32[1,512]{1,0:T(1,128)} %bitcast.5, ...), custom_call_target="tpu_custom_call" | custom-call | tf_op jit(solution)/shard_map/pallas_call | solution.py:564
  60.4 0.8 %copy.15 = bf16[64,4096]{1,0:T(8,128)(2,1)} copy(bf16[64,4096]{1,0:T(8,128)(2,1)S(1)} %shard_map.127) | data formatting | bytes 1048576

commit v5 on v4

--- a/solution.py
+++ b/solution.py
@@ -334,7 +334,7 @@
             seen = jnp.logical_and(seen, jnp.logical_and(u > 0, u < STEPS - 1))
         return bb * 4 + aa, spot, seen
 
-    def expand(sets):
+    def attend(sets, spot):
         keys = len(sets) * GROUP
         parts, rots = [], []
         for s in sets:
@@ -350,13 +350,7 @@
         latents = jnp.concatenate(parts, axis=0)
         kbuf[:keys, 0:512] = jnp.dot(latents, wuk[...], preferred_element_type=f32).astype(bf16)
         kbuf[:keys, 512:640] = jnp.concatenate(rots, axis=0)
-        values = lax.dot_general(
-            uvt[...], latents, (((1,), (1,)), ((), ())), preferred_element_type=f32
-        ).astype(bf16)
-        for h in range(HEADS):
-            vbuf[h, 0:VDIM, :keys] = values[h * VDIM : (h + 1) * VDIM]
-
-    def attend(keys, spot):
+
         def score(h):
             key = jnp.concatenate(
                 [kbuf[:keys, h * NOPE : (h + 1) * NOPE], kbuf[:keys, 512:640]], axis=1
@@ -371,6 +365,11 @@
             tops[h % 2] = jnp.max(scores, axis=0, keepdims=True)
 
         score(0)
+        values = lax.dot_general(
+            uvt[...], latents, (((1,), (1,)), ((), ())), preferred_element_type=f32
+        ).astype(bf16)
+        for h in range(HEADS):
+            vbuf[h, 0:VDIM, :keys] = values[h * VDIM : (h + 1) * VDIM]
         for h in range(HEADS):
             if h + 1 < HEADS:
                 score(h + 1)
@@ -386,6 +385,15 @@
     start(B1[2, 0], B1[2, 1])
     arrived(B1[1, 0], B1[1, 1])
     start(B2[1, 0])
+    arrived(QX)
+    for h in range(HEADS):
+        for j in range(2):
+            cols = slice(j * GROUP, (j + 1) * GROUP)
+            qfull[h, 0:NOPE, cols] = qt[j, h * NOPE : (h + 1) * NOPE, :]
+            at_row = HEADS * NOPE + h * ROPE
+            qfull[h, NOPE : NOPE + ROPE, cols] = qt[j, at_row : at_row + ROPE, :]
+        qfull[h, NOPE + ROPE :, :] = jnp.zeros((ROPE, 2 * GROUP), bf16)
+
     def far_seen(oa):
         aa, bb = mod4(a + oa), mod4(b + 2)
         return jnp.where(first, bb * 4 + aa, aa * 4 + bb) <= m
@@ -418,6 +426,11 @@
             arrived(B1[-1, -1], B1[-1, 2])
             start(B2[-1, 1])
 
+        @once(u == 6)
+        def _():
+            arrived(B1[2, -1], B1[2, 2])
+            start(B2[2, 1])
+
         for oa, when in ((0, 5), (1, 7), (-1, 7), (2, 8)):
 
             @once(jnp.logical_and(u == when, far_seen(oa)))
@@ -433,37 +446,11 @@
 
         @pl.when(two)
         def _():
-            expand((set_one, set_two))
+            attend((set_one, set_two), None)
 
         @pl.when(one)
         def _():
-            expand((single,))
-
-
-        @once(u == 0)
-        def _():
-            arrived(QX)
-            for h in range(HEADS):
-                for j in range(2):
-                    cols = slice(j * GROUP, (j + 1) * GROUP)
-                    qfull[h, 0:NOPE, cols] = qt[j, h * NOPE : (h + 1) * NOPE, :]
-                    at_row = HEADS * NOPE + h * ROPE
-                    qfull[h, NOPE : NOPE + ROPE, cols] = qt[j, at_row : at_row + ROPE, :]
-                qfull[h, NOPE + ROPE :, :] = jnp.zeros((ROPE, 2 * GROUP), bf16)
-
-        @once(u == 5)
-        def _():
-            arrived(B1[2, -1], B1[2, 2])
-            start(B2[2, 1])
-
-
-        @pl.when(two)
-        def _():
-            attend(2 * GROUP, None)
-
-        @pl.when(one)
-        def _():
-            attend(GROUP, spot)
+            attend((single,), spot)
 
         return carry
 

time: 61.3 us -> 60 us (0.979)
  Pallas kernels: 60.4 us -> 59 us
    pallas_call x1, Pallas kernels: 60.4 us -> 59 us  [local(): pl.pallas_call(kernel, out_shape=pltpu.VMEM((OWN, 4096), bf16), in_specs=...]
where the time goes in v5:
time: 60 us; the launch traced here: 59.9 us
  Pallas kernels  59 us (98%)
  local copies, waits for them, and re-layouts  0.8 us (1%)
    pallas_call x1, Pallas kernels, local(): pl.pallas_call(kernel, out_shape=pltpu.VMEM((OWN, 4096), bf16), in_specs=...  59 us

profile of v5, /device:TPU:96, one launch (start us, length us, event | category | flops | bytes accessed | tf_op | source)
XLA Modules:
  0.0 59.9 jit_solution(16785958016536094188)
XLA Ops:
  0.0 59.0 %shard_map.127 = bf16[64,4096]{1,0:T(8,128)(2,1)S(1)} custom-call(bf16[64,4096]{1,0:T(8,128)(2,1)} %tokens_in.1, bf16[4096,1024]{1,0:T(8,128)(2,1)} %down_query.1, bf16[4096,512]{1,0:T(8,128)(2,1)} %down_latent.1, bf16[64,4096]{1,0:T(8,128)(2,1)} %bitcast.3, f32[1,1024]{1,0:T(1,128)} %bitcast.4, f32[1,512]{1,0:T(1,128)} %bitcast.5, ...), custom_call_target="tpu_custom_call" | custom-call | tf_op jit(solution)/shard_map/pallas_call | solution.py:551
  59.1 0.8 %copy.15 = bf16[64,4096]{1,0:T(8,128)(2,1)} copy(bf16[64,4096]{1,0:T(8,128)(2,1)S(1)} %shard_map.127) | data formatting | bytes 1048576

commit v6 on v5

--- a/solution.py
+++ b/solution.py
@@ -27,7 +27,7 @@
 MESH = pl.DeviceIdType.MESH
 
 COLS = 4
-N_MSG = 102 + 6 * (COLS - 4)
+N_MSG = 103 + 6 * (COLS - 4)
 
 STEPS = 9
 UNIT_OA = ((0, 1, 0, 2, 1, -1, 2, 1, 2), (0, -1, 0, 1, -1, 0, 2, -1, 2))
@@ -234,7 +234,11 @@
         add(ql.at[xm, q_lo], ql.at[xm, q_lo], ql.at[x2, q_lo], dev_xp),
         add(ql.at[xp, q_hi], ql.at[xp, q_hi], ql.at[x2, q_hi], dev_xm),
     )
-    QX = (add(qt.at[c], qt.at[c], qt.at[1 - c], dev_core),)
+    QX = []
+    for n in range(2):
+        half = pl.ds(n * 2 * OWN, 2 * OWN)
+        mine = qt.at[c, :, half]
+        QX.append((add(mine, mine, qt.at[1 - c, :, half], dev_core),))
     OX = [(add(xsend.at[h], xrecv.at[h], xrecv.at[h], dev_core),) for h in range(HEADS)]
     OS = (add(ssend, srecv, srecv, dev_core),)
 
@@ -247,6 +251,13 @@
         for ids in groups:
             for i in ids:
                 recv[i].wait_recv()
+
+    def token_of(col):
+        place = col
+        for r, o in enumerate(OFFS):
+            inside = jnp.logical_and(col >= r * OWN, col < (r + 1) * OWN)
+            place = jnp.where(inside, col + (xs(o) - r) * OWN, place)
+        return place
 
     def norm_rows(values, gain):
         return values * lax.rsqrt(jnp.mean(values * values, axis=-1, keepdims=True) + norm_eps) * gain
@@ -284,20 +295,20 @@
         query = query + jnp.dot(tokens[:, cols], wdq[cols, :], preferred_element_type=f32)
     load_qgain.wait()
     ql[x] = norm_rows(query, qgain[...]).astype(bf16)
-    start(*Q1)
+    start(Q1[0])
     arrived(X1[0])
-    start(X2)
+    start(X2, Q1[1])
     arrived(X1[1])
     start(A1[1], A1[-1], B1[0, 1], B1[0, -1])
     load_rows.wait()
     for load in load_rest:
         load.wait()
-    uvt[...] = jnp.transpose(wuv[...].astype(f32)).astype(bf16)
+    uvt[...] = jnp.transpose(wuv[...])
     for h in range(HEADS):
         vbuf[h, VDIM:VROWS, :] = jnp.ones((VROWS - VDIM, 2 * GROUP), bf16)
     acc[...] = jnp.zeros_like(acc)
     best[...] = jnp.full(best.shape, masked_score, f32)
-    spot = lax.broadcasted_iota(jnp.int32, (32, GROUP), 1) + sp * GROUP
+    spot = token_of(lax.broadcasted_iota(jnp.int32, (32, GROUP), 1)) + sp * GROUP
     angles = spot.astype(f32) * rrate[...]
     cosine, sine = jnp.cos(angles), jnp.sin(angles)
     arrived(A1[0])
@@ -312,19 +323,30 @@
     start(A1[2], B1[0, 2])
     arrived(A1[-1])
     start(B1[1, -1], B1[-1, -1])
-    arrived(Q1[1], Q2)
     factor = (NOPE + ROPE) ** (-0.5) * 1.4426950408889634
-    rows = ql[...].reshape(GROUP, 1024)
-    plain = jnp.dot(rows, wuq[...], preferred_element_type=f32) * factor
-    qt[c, 0 : HEADS * NOPE, :] = jnp.transpose(plain).astype(bf16)
-    turned = jnp.transpose(jnp.dot(rows, wur[...], preferred_element_type=f32) * factor)
-    for h in range(HEADS):
-        one = turned[h * ROPE : h * ROPE + 32]
-        two = turned[h * ROPE + 32 : (h + 1) * ROPE]
-        at_row = HEADS * NOPE + h * ROPE
-        qt[c, at_row : at_row + 32, :] = (one * cosine - two * sine).astype(bf16)
-        qt[c, at_row + 32 : at_row + 64, :] = (two * cosine + one * sine).astype(bf16)
-    start(QX)
+
+    def make_queries(n):
+        half = slice(n * 2 * OWN, (n + 1) * 2 * OWN)
+        rows = jnp.concatenate([ql[xs(OFFS[2 * n])], ql[xs(OFFS[2 * n + 1])]], axis=0)
+        plain = jnp.dot(rows, wuq[...], preferred_element_type=f32) * factor
+        qt[c, 0 : HEADS * NOPE, half] = jnp.transpose(plain.astype(bf16))
+        turned = jnp.transpose(jnp.dot(rows, wur[...], preferred_element_type=f32) * factor)
+        for h in range(HEADS):
+            one = turned[h * ROPE : h * ROPE + 32]
+            two = turned[h * ROPE + 32 : (h + 1) * ROPE]
+            at_row = HEADS * NOPE + h * ROPE
+            qt[c, at_row : at_row + 32, half] = (
+                one * cosine[:, half] - two * sine[:, half]
+            ).astype(bf16)
+            qt[c, at_row + 32 : at_row + 64, half] = (
+                two * cosine[:, half] + one * sine[:, half]
+            ).astype(bf16)
+        start(QX[n])
+
+    arrived(Q1[1])
+    make_queries(0)
+    arrived(Q2)
+    make_queries(1)
 
     def set_of(u, n):
         aa, bb = mod4(a + pick(u, UNIT_OA[n])), mod4(b + pick(u, UNIT_OB[n]))
@@ -358,9 +380,10 @@
             scores = jnp.dot(key, qfull[h], preferred_element_type=f32)
             if spot is not None:
                 row = lax.broadcasted_iota(jnp.int32, (keys, 2 * GROUP), 0)
-                col = lax.broadcasted_iota(jnp.int32, (keys, 2 * GROUP), 1)
+                col = lax.broadcasted_iota(jnp.int32, (1, 2 * GROUP), 1)
+                col = jnp.where(col < GROUP, token_of(col), token_of(col - GROUP) + GROUP)
                 ahead = (2 * (spot - m) + c) * GROUP
-                scores = jnp.where(row + ahead <= col, scores, masked_score)
+                scores = jnp.where(row <= col - ahead, scores, masked_score)
             sbuf[h % 2, :keys] = scores
             tops[h % 2] = jnp.max(scores, axis=0, keepdims=True)
 
@@ -385,7 +408,7 @@
     start(B1[2, 0], B1[2, 1])
     arrived(B1[1, 0], B1[1, 1])
     start(B2[1, 0])
-    arrived(QX)
+    arrived(*QX)
     for h in range(HEADS):
         for j in range(2):
             cols = slice(j * GROUP, (j + 1) * GROUP)
@@ -474,7 +497,7 @@
         total = acc[h, 128:129, mine_at] * w_mine + srecv[h, 1:2, :] * w_theirs
         arrived(OX[h])
         summed = acc[h, 0:128, mine_at] * w_mine + xrecv[h].astype(f32) * w_theirs
-        heads.append(jnp.transpose(summed / total).astype(bf16))
+        heads.append(jnp.transpose((summed * (1.0 / total)).astype(bf16)))
     attended = jnp.concatenate(heads, axis=1)
 
     WIDE = 4096 // COLS
@@ -487,8 +510,8 @@
             up, down = ref.at[0, :, cols], ref.at[1, :, cols]
             return add(to_up, up, up, dev_xp), add(to_down, down, down, dev_xm)
 
-        R1.append(both(pbuf.at[x2, top, cols], pbuf.at[x2, low, cols], r1buf))
-        RD.append(both(pbuf.at[xp, low, cols], pbuf.at[xm, top, cols], dbuf))
+        R1.append(both(pbuf.at[3, top, cols], pbuf.at[3, low, cols], r1buf))
+        RD.append(both(pbuf.at[1, low, cols], pbuf.at[2, top, cols], dbuf))
         RC.append(both(cbuf.at[0, :, cols], cbuf.at[1, :, cols], crecv))
     assert len(send) == N_MSG, len(send)
     for k in range(COLS):
@@ -501,22 +524,22 @@
         cols = slice(k * WIDE, (k + 1) * WIDE)
         arrived(R1[k])
         cbuf[0, :, cols] = (
-            r1buf[0, :, cols].astype(f32) + pbuf[xp, 0:32, cols].astype(f32)
+            r1buf[0, :, cols].astype(f32) + pbuf[1, 0:32, cols].astype(f32)
         ).astype(bf16)
         cbuf[1, :, cols] = (
-            r1buf[1, :, cols].astype(f32) + pbuf[xm, 32:64, cols].astype(f32)
+            r1buf[1, :, cols].astype(f32) + pbuf[2, 32:64, cols].astype(f32)
         ).astype(bf16)
         start(RC[k])
     for k in range(COLS):
         cols = slice(k * WIDE, (k + 1) * WIDE)
         arrived(RD[k], RC[k])
         out[0:32, cols] = (
-            pbuf[x, 0:32, cols].astype(f32)
+            pbuf[0, 0:32, cols].astype(f32)
             + crecv[0, :, cols].astype(f32)
             + dbuf[1, :, cols].astype(f32)
         ).astype(bf16)
         out[32:64, cols] = (
-            pbuf[x, 32:64, cols].astype(f32)
+            pbuf[0, 32:64, cols].astype(f32)
             + crecv[1, :, cols].astype(f32)
             + dbuf[0, :, cols].astype(f32)
         ).astype(bf16)

time: 60 us -> 59.9 us (level)
  no operation moved by 1% of the time
where the time goes in v6:
time: 59.9 us; the launch traced here: 59.8 us
  Pallas kernels  59 us (98%)
  local copies, waits for them, and re-layouts  0.8 us (1%)
    pallas_call x1, Pallas kernels, local(): pl.pallas_call(kernel, out_shape=pltpu.VMEM((OWN, 4096), bf16), in_specs=...  59 us

profile of v6, /device:TPU:96, one launch (start us, length us, event | category | flops | bytes accessed | tf_op | source)
XLA Modules:
  0.0 59.8 jit_solution(2845715392599060916)
XLA Ops:
  0.0 59.0 %shard_map.127 = bf16[64,4096]{1,0:T(8,128)(2,1)S(1)} custom-call(bf16[64,4096]{1,0:T(8,128)(2,1)} %tokens_in.1, bf16[4096,1024]{1,0:T(8,128)(2,1)} %down_query.1, bf16[4096,512]{1,0:T(8,128)(2,1)} %down_latent.1, bf16[64,4096]{1,0:T(8,128)(2,1)} %bitcast.3, f32[1,1024]{1,0:T(1,128)} %bitcast.4, f32[1,512]{1,0:T(1,128)} %bitcast.5, ...), custom_call_target="tpu_custom_call" | custom-call | tf_op jit(solution)/shard_map/pallas_call | solution.py:574
  59.0 0.8 %copy.15 = bf16[64,4096]{1,0:T(8,128)(2,1)} copy(bf16[64,4096]{1,0:T(8,128)(2,1)S(1)} %shard_map.127) | data formatting | bytes 1048576

commit v7 on v6

--- a/solution.py
+++ b/solution.py
@@ -404,10 +404,14 @@
                 vbuf[h, :, :keys], weights, preferred_element_type=f32
             )
 
-    arrived(A2[0])
-    start(B1[2, 0], B1[2, 1])
-    arrived(B1[1, 0], B1[1, 1])
-    start(B2[1, 0])
+    def pass_second():
+        arrived(A2[0])
+        start(B1[2, 0], B1[2, 1])
+        arrived(B1[1, 0], B1[1, 1])
+        start(B2[1, 0])
+
+    once(jnp.logical_not(first))(pass_second)
+
     arrived(*QX)
     for h in range(HEADS):
         for j in range(2):
@@ -427,6 +431,7 @@
         def _():
             arrived(A1[2])
             start(A2[1], B1[1, 2], B1[-1, 2])
+            once(first)(pass_second)
             arrived(B1[-1, 0], B1[-1, 1])
             start(B2[-1, 0])
 

time: 59.9 us -> 59.9 us (level)
  no operation moved by 1% of the time
where the time goes in v7:
time: 59.9 us; the launch traced here: 59.8 us
  Pallas kernels  59 us (98%)
  local copies, waits for them, and re-layouts  0.8 us (1%)
    pallas_call x1, Pallas kernels, local(): pl.pallas_call(kernel, out_shape=pltpu.VMEM((OWN, 4096), bf16), in_specs=...  59 us

profile of v7, /device:TPU:96, one launch (start us, length us, event | category | flops | bytes accessed | tf_op | source)
XLA Modules:
  0.0 59.8 jit_solution(3567089307122373206)
XLA Ops:
  0.0 59.0 %shard_map.127 = bf16[64,4096]{1,0:T(8,128)(2,1)S(1)} custom-call(bf16[64,4096]{1,0:T(8,128)(2,1)} %tokens_in.1, bf16[4096,1024]{1,0:T(8,128)(2,1)} %down_query.1, bf16[4096,512]{1,0:T(8,128)(2,1)} %down_latent.1, bf16[64,4096]{1,0:T(8,128)(2,1)} %bitcast.3, f32[1,1024]{1,0:T(1,128)} %bitcast.4, f32[1,512]{1,0:T(1,128)} %bitcast.5, ...), custom_call_target="tpu_custom_call" | custom-call | tf_op jit(solution)/shard_map/pallas_call | solution.py:579
  59.0 0.8 %copy.15 = bf16[64,4096]{1,0:T(8,128)(2,1)} copy(bf16[64,4096]{1,0:T(8,128)(2,1)S(1)} %shard_map.127) | data formatting | bytes 1048576

commit v8 on v7

--- a/solution.py
+++ b/solution.py
@@ -535,6 +535,17 @@
             r1buf[1, :, cols].astype(f32) + pbuf[2, 32:64, cols].astype(f32)
         ).astype(bf16)
         start(RC[k])
+    for oa in OFFS:
+
+        @pl.when(jnp.logical_not(far_seen(oa)))
+        def _(oa=oa):
+            arrived(B2[oa, 0], B2[oa, 1])
+
+    tail = [i for ids in (*RD, *RC) for i in ids]
+    for i in range(N_MSG):
+        if i not in tail:
+            send[i].wait_send()
+
     for k in range(COLS):
         cols = slice(k * WIDE, (k + 1) * WIDE)
         arrived(RD[k], RC[k])
@@ -548,13 +559,7 @@
             + crecv[1, :, cols].astype(f32)
             + dbuf[0, :, cols].astype(f32)
         ).astype(bf16)
-    for oa in OFFS:
-
-        @pl.when(jnp.logical_not(far_seen(oa)))
-        def _(oa=oa):
-            arrived(B2[oa, 0], B2[oa, 1])
-
-    for i in range(N_MSG):
+    for i in tail:
         send[i].wait_send()
 
 

time: 59.9 us -> 59.7 us (level)
  no operation moved by 1% of the time
where the time goes in v8:
time: 59.7 us; the launch traced here: 59.6 us
  Pallas kernels  58.8 us (98%)
  local copies, waits for them, and re-layouts  0.8 us (1%)
    pallas_call x1, Pallas kernels, local(): pl.pallas_call(kernel, out_shape=pltpu.VMEM((OWN, 4096), bf16), in_specs=...  58.8 us

profile of v8, /device:TPU:96, one launch (start us, length us, event | category | flops | bytes accessed | tf_op | source)
XLA Modules:
  0.0 59.6 jit_solution(6500168915353274700)
XLA Ops:
  0.0 58.8 %shard_map.127 = bf16[64,4096]{1,0:T(8,128)(2,1)S(1)} custom-call(bf16[64,4096]{1,0:T(8,128)(2,1)} %tokens_in.1, bf16[4096,1024]{1,0:T(8,128)(2,1)} %down_query.1, bf16[4096,512]{1,0:T(8,128)(2,1)} %down_latent.1, bf16[64,4096]{1,0:T(8,128)(2,1)} %bitcast.3, f32[1,1024]{1,0:T(1,128)} %bitcast.4, f32[1,512]{1,0:T(1,128)} %bitcast.5, ...), custom_call_target="tpu_custom_call" | custom-call | tf_op jit(solution)/shard_map/pallas_call | solution.py:584
  58.9 0.8 %copy.15 = bf16[64,4096]{1,0:T(8,128)(2,1)} copy(bf16[64,4096]{1,0:T(8,128)(2,1)S(1)} %shard_map.127) | data formatting | bytes 1048576
